TPU v7x, 256 devices: a whole 4x4x8 slice. The times are simulated.
256 devices in a mesh: vp: 32 (over z, x), dp: 8 (over y, core).
Axes of the slice: x: 4, y: 4, z: 8, core: 2. Of those that a mesh axis runs over, the one named last changes fastest.
Arguments:
- hidden_rows: bfloat16 [768, 8, 2048], P('vp', 'dp'), may hold values from -48 to 48
- norm_gain: float32 [2048], replicated, may hold values from 0.1 to 1.9
- vocab_matrix: bfloat16 [2048, 32768], P(None, 'vp'), may hold values from -3 to 3
- vocab_bias: float32 [32768], P('vp'), may hold values from -4 to 4
- targets: int32 [768, 8], P(None, 'dp'), may hold values from 0 to 32767
- loss_weight: float32 [768, 8], P(None, 'dp'), may hold values from 0.5 to 8
Outputs:
- losses: float32 [768, 8], P('vp', 'dp')
- norm_grad: float32 [768, 8, 2048], P('vp', 'dp')
- vocab_grad: float32 [2048, 32768], P('dp', 'vp')
All inputs are finite; a program needn't handle non-finite values.
Results may differ from a plain program's by a relative error of at most 0.0056.
Values may be sent and summed in bfloat16 or wider, within the bound.
No kernel may reach another device: no remote copies, remote signals or barrier semaphores. Data moves between devices by JAX's collectives and lax.ppermute only.
A program may use at most 64 MiB of HBM per device.

v0:
```python
import jax
import jax.numpy as jnp
import numpy as np
from jax import lax
from jax.experimental import pallas as pl
from jax.experimental.pallas import tpu as pltpu
from jax.sharding import Mesh
from jax.sharding import PartitionSpec as P


VP = ("vp_0", "vp_1")
DP = ("dp_0", "dp_1")


epsilon = 1e-06
penalty = 0.005
f32 = jnp.float32
bf16 = jnp.bfloat16

NZ, NX, NY, NC = 8, 4, 4, 2
FAR = (3, 4, 5)


def taken_from(array, axis, step):
    count = lax.axis_size(axis)
    return lax.ppermute(array, axis, [(i, (i - step) % count) for i in range(count)])


def sent_to(array, axis, step):
    return taken_from(array, axis, -step)


def slots(own):
    near = [(kz, kx) for kz in (0, 1, 7) for kx in range(NX)]
    far = [(kz, kx) for kx in range(NX) for kz in FAR]
    ring = [(kz, kx) for kz in (2, 6) for kx in range(NX)]
    return np.array([(kz, kx, r) for kz, kx in near + far + ring for r in range(own)], np.int32)


def three_parts(values):
    high = lax.reduce_precision(values, 8, 7)
    middle = lax.reduce_precision(values - high, 8, 7)
    low = values - high - middle
    return [part.astype(bf16) for part in (high, middle, low)]


def moved(matrix, vectors, dims):
    parts = jnp.stack([part for vector in vectors for part in three_parts(vector)])
    out = lax.dot_general(parts, matrix, (((1,), dims), ((), ())), preferred_element_type=f32)
    return [out[k] + out[k + 1] + out[k + 2] for k in range(0, 3 * len(vectors), 3)]


def column_vectors(order, vectors):
    high = vectors.astype(bf16)
    left = vectors - high.astype(f32)
    middle = left.astype(bf16)
    low = (left - middle.astype(f32)).astype(bf16)
    return sum(
        lax.dot_general(order, part, (((1,), (1,)), ((), ())), preferred_element_type=f32)
        for part in (high, middle, low)
    )


def gradient_kernel(
    scores, matrix, order, vectors, grad, far_own, near, upward, downward, *far_away
):
    columns = column_vectors(order[...], vectors[...])
    log_total, weights, target = columns[:, 0:1], columns[:, 1:2], columns[:, 2:3]
    scale = weights * (1.0 + 2.0 * penalty * log_total)
    target = target.astype(jnp.int32)
    rows, width = scores.shape
    step = 256
    for low in range(0, width, step):
        part = slice(low, low + step)
        ids = lax.broadcasted_iota(jnp.int32, (rows, step), 1) + low
        probs = jnp.exp(scores[:, part] - log_total)
        grad[:, part] = (
            scale * probs - jnp.where(ids == target, weights, 0.0)
        ).astype(bf16)

    block, wide = upward.shape[0], far_own.shape[0]

    def body(number, carry):
        part = pl.ds(pl.multiple_of(number * step, step), step)
        out = lax.dot_general(
            grad[...], matrix[part, :], (((1,), (1,)), ((), ())), preferred_element_type=f32
        )
        near[:, part] = out[: 3 * block]
        at = 3 * block
        far_own[:, part] = out[at : at + wide]
        for ref in far_away:
            at += wide
            ref[:, part] = out[at : at + wide].astype(bf16)
        at += wide
        upward[:, part] = out[at : at + block].astype(bf16)
        downward[:, part] = out[at + block :].astype(bf16)
        return carry

    lax.fori_loop(0, matrix.shape[0] // step, body, 0)


def vocab_product(rows, grad, first, share):
    part = pl.ds(pl.multiple_of(first * share, share), share)
    return lax.dot_general(
        rows[:, part], grad[...], (((0,), (0,)), ((), ())), preferred_element_type=f32
    )


def other_kernel(place, rows, grad, out):
    share = rows.shape[1] // (NY * NC)

    def body(y, carry):
        product = vocab_product(rows, grad, y * NC + 1 - place[1], share)
        out[pl.ds(pl.multiple_of(y * share, share), share), :] = product.astype(bf16)
        return carry

    lax.fori_loop(0, NY, body, 0)


def chip_kernel(place, rows, grad, other, own, *away):
    share = rows.shape[1] // (NY * NC)
    for k, ref in enumerate((own, *away)):
        y = lax.rem(place[0] + k, NY)
        product = vocab_product(rows, grad, y * NC + place[1], share)
        product = product + other[pl.ds(pl.multiple_of(y * share, share), share), :].astype(f32)
        ref[...] = product.astype(ref.dtype)


def shaped(*shapes):
    return tuple(jax.ShapeDtypeStruct(dims, kind) for dims, kind in shapes)


def spaces(scalars, arrays):
    return [pl.BlockSpec(memory_space=pltpu.SMEM)] * scalars + [
        pl.BlockSpec(memory_space=pltpu.VMEM)
    ] * arrays


def whole(hidden_rows, norm_gain, vocab_matrix, vocab_bias, targets, loss_weight):
    inputs = hidden_rows[:, 0, :].astype(f32)
    inverse_rms = lax.rsqrt(jnp.mean(inputs * inputs, axis=-1, keepdims=True) + epsilon)
    unit_rows = inputs * inverse_rms
    normed = (unit_rows * norm_gain).astype(bf16)
    own, width = normed.shape
    total_rows = own * NZ * NX
    columns = vocab_matrix.shape[1]

    along_x = {kx: taken_from(normed, "vp_1", kx) for kx in (1, 3, 2)}
    straight = {kz: taken_from(normed, "vp_0", kz) for kz in (4, 3, 5)}
    line = jnp.concatenate([normed] + [along_x[kx] for kx in range(1, NX)])
    up1 = taken_from(line, "vp_0", 1)
    down1 = taken_from(line, "vp_0", -1)
    three = lax.optimization_barrier(jnp.concatenate([straight[kz] for kz in FAR]))
    threes = {kx: taken_from(three, "vp_1", kx) for kx in (2, 1, 3)}
    up2 = taken_from(up1, "vp_0", 1)
    down2 = taken_from(down1, "vp_0", -1)
    rows_all = jnp.concatenate(
        [line, up1, down1, three] + [threes[kx] for kx in range(1, NX)] + [up2, down2]
    )

    place_z, place_x = lax.axis_index("vp_0"), lax.axis_index("vp_1")
    place = slots(own)
    owner = (place_z + place[:, 0]) % NZ * NX + (place_x + place[:, 1]) % NX
    index = owner * own + place[:, 2]
    ids = lax.broadcasted_iota(jnp.int32, (total_rows, total_rows), 1)
    order = (index[:, None] == ids).astype(bf16)

    target_col, _ = moved(
        order, [targets[:, 0].astype(f32), loss_weight[:, 0]], (1,)
    )
    target_col = target_col.astype(jnp.int32) - lax.axis_index(VP) * columns
    column_ids = lax.broadcasted_iota(jnp.int32, (total_rows, columns), 1)
    is_target = column_ids == target_col[:, None]

    scores = jnp.dot(rows_all, vocab_matrix, preferred_element_type=f32) + vocab_bias[None, :]
    maxima = jnp.max(scores, axis=1)
    totals = jnp.sum(jnp.exp(scores - maxima[:, None]), axis=1)
    target_score = jnp.sum(jnp.where(is_target, scores, 0.0), axis=1)
    partial_log, target_score = moved(order, [maxima + jnp.log(totals), target_score], (0,))
    count = NZ * NX
    target_score = jnp.pad(target_score.reshape(count, own), ((0, 0), (0, 128 - own)))
    packed = jnp.concatenate(
        [jnp.broadcast_to(partial_log, (count, total_rows)), target_score], axis=1
    )[:, None, :]
    packed = lax.all_to_all(packed, VP, split_axis=0, concat_axis=0, tiled=True)[:, 0]
    each = packed[:, :total_rows]
    maxima = jnp.max(each, axis=0)
    log_total = maxima + jnp.log(jnp.sum(jnp.exp(each - maxima), axis=0))
    own_log = lax.dynamic_slice_in_dim(log_total, lax.axis_index(VP) * own, own)
    own_target = jnp.sum(packed[:, total_rows : total_rows + own], axis=0)
    own_loss = own_log - own_target + penalty * own_log * own_log
    first = lax.axis_index(VP) * columns
    vectors = jnp.concatenate(
        [
            log_total[None],
            loss_weight.T,
            (targets.T - first).astype(f32),
            jnp.zeros((5, total_rows), f32),
        ]
    )
    block = NX * own
    wide = len(FAR) * own
    score_grad, far_own, near, upward, downward, *far_away = pl.pallas_call(
        gradient_kernel,
        out_shape=shaped(
            ((total_rows, columns), bf16),
            ((wide, width), f32),
            ((3 * block, width), f32),
            ((block, width), bf16),
            ((block, width), bf16),
            *[((wide, width), bf16)] * (NX - 1),
        ),
        in_specs=spaces(0, 4),
        out_specs=spaces(0, 5 + NX - 1),
    )(scores, vocab_matrix, order, vectors)
    from_below = sent_to(upward, "vp_0", 1)
    from_above = sent_to(downward, "vp_0", -1)
    far_x = {kx: sent_to(far_away[kx - 1], "vp_1", kx) for kx in (2, 1, 3)}

    share = width // (NY * NC)
    place = jnp.stack([lax.axis_index("dp_0"), lax.axis_index("dp_1")])
    (other,) = pl.pallas_call(
        other_kernel,
        out_shape=shaped(((NY * share, columns), bf16)),
        in_specs=spaces(1, 2),
        out_specs=spaces(0, 1),
    )(place, rows_all, score_grad)
    other = taken_from(other, "dp_1", 1)
    vocab_grad, *away = pl.pallas_call(
        chip_kernel,
        out_shape=shaped(
            ((share, columns), f32), *[((share, columns), bf16)] * (NY - 1)
        ),
        in_specs=spaces(1, 3),
        out_specs=spaces(0, NY),
    )(place, rows_all, score_grad, other)
    chip_y = {k: sent_to(away[k - 1], "dp_0", k) for k in (2, 1, 3)}
    above, below = near[block : 2 * block], near[2 * block :]
    from_below = sent_to((above + from_below.astype(f32)).astype(bf16), "vp_0", 1)
    from_above = sent_to((below + from_above.astype(f32)).astype(bf16), "vp_0", -1)
    far_sum = far_own
    for kx in range(1, NX):
        far_sum = far_sum + far_x[kx].astype(f32)
    far_sum = far_sum.astype(bf16)
    arrived = [sent_to(far_sum[k * own : (k + 1) * own], "vp_0", FAR[k]) for k in (1, 0, 2)]
    close = near[:block] + from_below.astype(f32) + from_above.astype(f32)
    close_half = close.astype(bf16)
    arrived += [sent_to(close_half[kx * own : (kx + 1) * own], "vp_1", kx) for kx in (2, 1, 3)]
    row_grad = close[:own]
    for piece in arrived:
        row_grad = row_grad + piece.astype(f32)

    scaled_grad = norm_gain * row_grad
    norm_grad = inverse_rms * (
        scaled_grad - unit_rows * jnp.mean(scaled_grad * unit_rows, axis=-1, keepdims=True)
    )
    for k in (2, 1, 3):
        vocab_grad = vocab_grad + chip_y[k].astype(f32)
    return (own_loss[:, None], norm_grad[:, None, :], vocab_grad)


def solution(mesh):
    split = Mesh(mesh.devices.reshape(8, 4, 4, 2), ("vp_0", "vp_1", "dp_0", "dp_1"))
    in_specs = (P(VP, DP, None), P(), P(None, VP), P(VP), P(None, DP), P(None, DP))
    out_specs = (P(VP, DP), P(VP, DP, None), P(DP, VP))
    return jax.shard_map(whole, mesh=split, in_specs=in_specs, out_specs=out_specs, check_vma=False)
```

profile of v0, /device:TPU:8, one launch (start us, length us, event | category | flops | bytes accessed | tf_op | source)
XLA Modules:
  0.0 169.6 jit_solution(14147016360366252795)
XLA Ops:
  2.7 4.7 %collective-permute-start.7 = (bf16[24,2048]{1,0:T(8,128)(2,1)S(1)}, bf16[24,2048]{1,0:T(8,128)(2,1)S(1)}, u32[]{:S(2)}, u32[]{:S(2)}) collective-permute-start(bf16[24,2048]{1,0:T(8,128)(2,1)S(1)} %get-tuple-element.45), channel_id=1, source_target_pairs={{0,96},{32,128},{64,160},{96,192},{128,224},{160,0},{192,32},{224,... | collective-permute-start | bytes 294920 | tf_op jit(solution)/shard_map/ppermute | solution.py:26
  7.4 4.5 %collective-permute-start.6 = (bf16[24,2048]{1,0:T(8,128)(2,1)S(1)}, bf16[24,2048]{1,0:T(8,128)(2,1)}, u32[]{:S(2)}, u32[]{:S(2)}) collective-permute-start(bf16[24,2048]{1,0:T(8,128)(2,1)S(1)} %get-tuple-element.45), channel_id=1, source_target_pairs={{0,128},{32,160},{64,192},{96,224},{128,0},{160,32},{192,64},{224,... | collective-permute-start | bytes 294920 | tf_op jit(solution)/shard_map/ppermute | solution.py:26
  11.9 3.1 %collective-permute-start.5 = (bf16[24,2048]{1,0:T(8,128)(2,1)S(1)}, bf16[24,2048]{1,0:T(8,128)(2,1)}, u32[]{:S(2)}, u32[]{:S(2)}) collective-permute-start(bf16[24,2048]{1,0:T(8,128)(2,1)S(1)} %get-tuple-element.45), channel_id=1, source_target_pairs={{0,160},{32,192},{64,224},{96,0},{128,32},{160,64},{192,96},{224,1... | collective-permute-start | bytes 294920 | tf_op jit(solution)/shard_map/ppermute | solution.py:26
  15.0 1.5 collective-permute-start.2
  16.5 2.7 %collective-permute-start.1 = (bf16[24,2048]{1,0:T(8,128)(2,1)S(1)}, bf16[24,2048]{1,0:T(8,128)(2,1)S(1)}, u32[]{:S(2)}, u32[]{:S(2)}) collective-permute-start(bf16[24,2048]{1,0:T(8,128)(2,1)S(1)} %get-tuple-element.45), channel_id=1, source_target_pairs={{0,16},{8,24},{16,0},{24,8},{1,17},{9,25},{17,1},{25,9},{2,18},{10... | collective-permute-start | bytes 294920 | tf_op jit(solution)/shard_map/ppermute | solution.py:26
  25.5 1.5 collective-permute-start
  29.6 1.9 %collective-permute-start.8 = (bf16[72,2048]{1,0:T(8,128)(2,1)S(1)}, bf16[72,2048]{1,0:T(8,128)(2,1)S(1)}, u32[]{:S(2)}, u32[]{:S(2)}) collective-permute-start(bf16[72,2048]{1,0:T(8,128)(2,1)S(1)} %pad_maximum_fusion.1), channel_id=1, source_target_pairs={{0,24},{8,0},{16,8},{24,16},{1,25},{9,1},{17,9},{25,17},{2,26},{10... | collective-permute-start | bytes 884744 | tf_op jit(solution)/shard_map/ppermute | solution.py:26
  31.5 2.2 %collective-permute-start.4 = (bf16[96,2048]{1,0:T(8,128)(2,1)S(1)}, bf16[96,2048]{1,0:T(8,128)(2,1)S(1)}, u32[]{:S(2)}, u32[]{:S(2)}) collective-permute-start(bf16[96,2048]{1,0:T(8,128)(2,1)S(1)} %pad_maximum_fusion), channel_id=1, source_target_pairs={{0,32},{32,64},{64,96},{96,128},{128,160},{160,192},{192,224},{224... | collective-permute-start | bytes 1179656 | tf_op jit(solution)/shard_map/ppermute | solution.py:26
  34.8 8.4 %collective-permute-done.3 = bf16[96,2048]{1,0:T(8,128)(2,1)S(1)} collective-permute-done((bf16[96,2048]{1,0:T(8,128)(2,1)S(1)}, bf16[96,2048]{1,0:T(8,128)(2,1)S(1)}, u32[]{:S(2)}, u32[]{:S(2)}) %collective-permute-start.3) | collective-permute-done | bytes 393248 | tf_op jit(solution)/shard_map/ppermute | solution.py:26
  43.8 2.9 %collective-permute-start.11 = (bf16[96,2048]{1,0:T(8,128)(2,1)S(1)}, bf16[96,2048]{1,0:T(8,128)(2,1)S(1)}, u32[]{:S(2)}, u32[]{:S(2)}) collective-permute-start(bf16[96,2048]{1,0:T(8,128)(2,1)S(1)} %collective-permute-done.3), channel_id=1, source_target_pairs={{0,224},{32,0},{64,32},{96,64},{128,96},{160,128},{192,160},{224,1... | collective-permute-start | bytes 1179656 | tf_op jit(solution)/shard_map/ppermute | solution.py:26
  46.8 5.8 %collective-permute-done.11 = bf16[96,2048]{1,0:T(8,128)(2,1)S(1)} collective-permute-done((bf16[96,2048]{1,0:T(8,128)(2,1)S(1)}, bf16[96,2048]{1,0:T(8,128)(2,1)S(1)}, u32[]{:S(2)}, u32[]{:S(2)}) %collective-permute-start.11) | collective-permute-done | bytes 393248 | tf_op jit(solution)/shard_map/ppermute | solution.py:26
  53.4 3.6 %fusion.42 = (f32[768]{0:T(1024)S(1)}, f32[768,1024]{1,0:T(8,128)S(1)}) fusion(f32[1024]{0:T(1024)S(1)} %copy-done.11, bf16[768,2048]{1,0:T(8,128)(2,1)S(1)} %constant_dynamic-update-slice_fusion.rows, bf16[2048,1024]{1,0:T(8,128)(2,1)S(1)} %copy-done.2), kind=kOutput, calls=%fused_computation.113 | convolution fusion | flops 3222797568 | bytes 10492928 | tf_op jit(solution)/shard_map/dot_general | solution.py:175
  57.0 1.6 copy-done.1
  61.3 4.7 %all-to-all-start = ((f32[32,1,896]{2,1,0:T(1,128)}), f32[32,1,896]{2,1,0:T(1,128)S(1)}, u32[]{:S(2)}, u32[]{:S(2)}) async-start(f32[32,1,896]{2,1,0:T(1,128)} %broadcast_in_dim.16), calls=%async_computation | async-start | bytes 229376 | tf_op jit(solution)/shard_map/all_to_all | solution.py:185
  66.0 10.3 %all-to-all-done = f32[32,1,896]{2,1,0:T(1,128)S(1)} async-done(((f32[32,1,896]{2,1,0:T(1,128)}), f32[32,1,896]{2,1,0:T(1,128)S(1)}, u32[]{:S(2)}, u32[]{:S(2)}) %all-to-all-start) | async-done | bytes 114720 | tf_op jit(solution)/shard_map/all_to_all | solution.py:185
  77.1 12.8 %shard_map.112 = (bf16[768,1024]{1,0:T(8,128)(2,1)}, f32[72,2048]{1,0:T(8,128)}, f32[288,2048]{1,0:T(8,128)}, bf16[96,2048]{1,0:T(8,128)(2,1)}, bf16[96,2048]{1,...) custom-call(f32[768,1024]{1,0:T(8,128)} %copy-done.1, ...), custom_call_target="tpu_custom_call" | custom-call | tf_op jit(solution)/shard_map/pallas_call | solution.py:203
  90.2 2.6 %collective-permute-start.18 = (bf16[72,2048]{1,0:T(8,128)(2,1)}, bf16[72,2048]{1,0:T(8,128)(2,1)}, u32[]{:S(2)}, u32[]{:S(2)}) collective-permute-start(bf16[72,2048]{1,0:T(8,128)(2,1)} %get-tuple-element.20), channel_id=1, source_target_pairs={{0,16},{8,24},{16,0},{24,8},{1,17},{9,25},{17,1},{25,9},{2,18},{10... | collective-permute-start | bytes 884744 | tf_op jit(solution)/shard_map/ppermute | solution.py:26
  95.1 2.6 %collective-permute-start.15 = (bf16[96,2048]{1,0:T(8,128)(2,1)}, bf16[96,2048]{1,0:T(8,128)(2,1)}, u32[]{:S(2)}, u32[]{:S(2)}) collective-permute-start(bf16[96,2048]{1,0:T(8,128)(2,1)} %get-tuple-element.17), channel_id=1, source_target_pairs={{0,224},{32,0},{64,32},{96,64},{128,96},{160,128},{192,160},{224,1... | collective-permute-start | bytes 1179656 | tf_op jit(solution)/shard_map/ppermute | solution.py:26
  97.7 6.4 %shard_map.113 = bf16[1024,1024]{1,0:T(8,128)(2,1)} custom-call(s32[2]{0:T(128)} %pad_add_fusion.place, bf16[768,2048]{1,0:T(8,128)(2,1)} %copy-done, bf16[768,1024]{1,0:T(8,128)(2,1)} %get-tuple-element.22.grad), custom_call_target="tpu_custom_call" | custom-call | tf_op jit(solution)/shard_map/pallas_call | solution.py:222
  107.2 3.2 %collective-permute-start.16 = (bf16[96,2048]{1,0:T(8,128)(2,1)S(1)}, bf16[96,2048]{1,0:T(8,128)(2,1)S(1)}, u32[]{:S(2)}, u32[]{:S(2)}) collective-permute-start(bf16[96,2048]{1,0:T(8,128)(2,1)S(1)} %get-tuple-element.47), channel_id=1, source_target_pairs={{0,224},{32,0},{64,32},{96,64},{128,96},{160,128},{192,160},{224,1... | collective-permute-start | bytes 1179656 | tf_op jit(solution)/shard_map/ppermute | solution.py:26
  111.6 2.2 %collective-permute-start.22 = (bf16[24,2048]{1,0:T(8,128)(2,1)S(1)}, bf16[24,2048]{1,0:T(8,128)(2,1)S(1)}, u32[]{:S(2)}, u32[]{:S(2)}) collective-permute-start(bf16[24,2048]{1,0:T(8,128)(2,1)S(1)} %get-tuple-element.52), channel_id=1, source_target_pairs={{0,160},{32,192},{64,224},{96,0},{128,32},{160,64},{192,96},{224,1... | collective-permute-start | bytes 294920 | tf_op jit(solution)/shard_map/ppermute | solution.py:26
  113.9 12.5 %collective-permute-done.14 = bf16[96,2048]{1,0:T(8,128)(2,1)S(1)} collective-permute-done((bf16[96,2048]{1,0:T(8,128)(2,1)S(1)}, bf16[96,2048]{1,0:T(8,128)(2,1)S(1)}, u32[]{:S(2)}, u32[]{:S(2)}) %collective-permute-start.14) | collective-permute-done | bytes 393248 | tf_op jit(solution)/shard_map/ppermute | solution.py:26
  126.5 2.4 %collective-permute-start.23 = (bf16[24,2048]{1,0:T(8,128)(2,1)S(1)}, bf16[24,2048]{1,0:T(8,128)(2,1)S(1)}, u32[]{:S(2)}, u32[]{:S(2)}) collective-permute-start(bf16[24,2048]{1,0:T(8,128)(2,1)S(1)} %get-tuple-element.48), channel_id=1, source_target_pairs={{0,16},{8,24},{16,0},{24,8},{1,17},{9,25},{17,1},{25,9},{2,18},{10... | collective-permute-start | bytes 294920 | tf_op jit(solution)/shard_map/ppermute | solution.py:26
  128.9 1.4 collective-permute-start.25
  131.6 2.4 %collective-permute-done.21 = bf16[24,2048]{1,0:T(8,128)(2,1)S(1)} collective-permute-done((bf16[24,2048]{1,0:T(8,128)(2,1)S(1)}, bf16[24,2048]{1,0:T(8,128)(2,1)S(1)}, u32[]{:S(2)}, u32[]{:S(2)}) %collective-permute-start.21) | collective-permute-done | bytes 98336 | tf_op jit(solution)/shard_map/ppermute | solution.py:26
  134.0 2.2 %collective-permute-done.24 = bf16[24,2048]{1,0:T(8,128)(2,1)S(1)} collective-permute-done((bf16[24,2048]{1,0:T(8,128)(2,1)S(1)}, bf16[24,2048]{1,0:T(8,128)(2,1)S(1)}, u32[]{:S(2)}, u32[]{:S(2)}) %collective-permute-start.24) | collective-permute-done | bytes 98336 | tf_op jit(solution)/shard_map/ppermute | solution.py:26
  136.4 5.7 %shard_map.114 = (f32[256,1024]{1,0:T(8,128)}, bf16[256,1024]{1,0:T(8,128)(2,1)}, bf16[256,1024]{1,0:T(8,128)(2,1)}, bf16[256,1024]{1,0:T(8,128)(2,1)}) custom-call(s32[2]{0:T(128)} %pad_add_fusion.place, bf16[768,2048]{1,0:T(8,128)(2,1)} %copy-done, bf16[768,1024]{1,0:T(8,128)(2,1)} %get-tuple-element.22.grad, bf16[1024,1024]{1,0:T(8,128)(2,1)} %collective-permute-done.26.other), custom_call_target="tpu_custom_call" | custom-call | tf_op jit(solution)/shard_map/pallas_call | solution.py:229
  142.1 2.3 %collective-permute-start.27 = (bf16[256,1024]{1,0:T(8,128)(2,1)}, bf16[256,1024]{1,0:T(8,128)(2,1)S(1)}, u32[]{:S(2)}, u32[]{:S(2)}) collective-permute-start(bf16[256,1024]{1,0:T(8,128)(2,1)} %get-tuple-element.24), channel_id=1, source_target_pairs={{0,4},{2,6},{4,0},{6,2},{1,5},{3,7},{5,1},{7,3},{8,12},{10,14},{12... | collective-permute-start | bytes 1572872 | tf_op jit(solution)/shard_map/ppermute | solution.py:26
  144.5 2.0 %collective-permute-start.29 = (bf16[256,1024]{1,0:T(8,128)(2,1)}, bf16[256,1024]{1,0:T(8,128)(2,1)S(1)}, u32[]{:S(2)}, u32[]{:S(2)}) collective-permute-start(bf16[256,1024]{1,0:T(8,128)(2,1)} %get-tuple-element.26), channel_id=1, source_target_pairs={{0,6},{2,0},{4,2},{6,4},{1,7},{3,1},{5,3},{7,5},{8,14},{10,8},{12,... | collective-permute-start | bytes 1572872 | tf_op jit(solution)/shard_map/ppermute | solution.py:26
  147.5 11.2 %collective-permute-done.27 = bf16[256,1024]{1,0:T(8,128)(2,1)S(1)} collective-permute-done((bf16[256,1024]{1,0:T(8,128)(2,1)}, bf16[256,1024]{1,0:T(8,128)(2,1)S(1)}, u32[]{:S(2)}, u32[]{:S(2)}) %collective-permute-start.27) | collective-permute-done | bytes 524320 | tf_op jit(solution)/shard_map/ppermute | solution.py:26
  158.6 8.4 %collective-permute-done.28 = bf16[256,1024]{1,0:T(8,128)(2,1)S(1)} collective-permute-done((bf16[256,1024]{1,0:T(8,128)(2,1)}, bf16[256,1024]{1,0:T(8,128)(2,1)S(1)}, u32[]{:S(2)}, u32[]{:S(2)}) %collective-permute-start.28) | collective-permute-done | bytes 524320 | tf_op jit(solution)/shard_map/ppermute | solution.py:26
  167.0 2.5 %convert_add_fusion = f32[256,1024]{1,0:T(8,128)} fusion(bf16[256,1024]{1,0:T(8,128)(2,1)S(1)} %collective-permute-done.29, bf16[256,1024]{1,0:T(8,128)(2,1)S(1)} %collective-permute-done.28, f32[256,1024]{1,0:T(8,128)} %get-tuple-element.23, bf16[256,1024]{1,0:T(8,128)(2,1)S(1)} %collective-permute-done.27), kind=kLoop, calls=%fused_computation.10 | loop fusion | flops 1572864 | bytes 3670016 | tf_op jit(solution)/shard_map/add | solution.py:258
  (113 shorter events, 26.1 us)
Async XLA Ops:
  2.7 22.8 %collective-permute-start.7 = (bf16[24,2048]{1,0:T(8,128)(2,1)S(1)}, bf16[24,2048]{1,0:T(8,128)(2,1)S(1)}, u32[]{:S(2)}, u32[]{:S(2)}) collective-permute-start(bf16[24,2048]{1,0:T(8,128)(2,1)S(1)} %get-tuple-element.45), channel_id=1, source_target_pairs={{0,96},{32,128},{64,160},{96,192},{128,224},{160,0},{192,32},{224,... | collective-permute-start | bytes 294920 | tf_op jit(solution)/shard_map/ppermute | solution.py:26
  7.4 19.6 %collective-permute-start.6 = (bf16[24,2048]{1,0:T(8,128)(2,1)S(1)}, bf16[24,2048]{1,0:T(8,128)(2,1)}, u32[]{:S(2)}, u32[]{:S(2)}) collective-permute-start(bf16[24,2048]{1,0:T(8,128)(2,1)S(1)} %get-tuple-element.45), channel_id=1, source_target_pairs={{0,128},{32,160},{64,192},{96,224},{128,0},{160,32},{192,64},{224,... | collective-permute-start | bytes 294920 | tf_op jit(solution)/shard_map/ppermute | solution.py:26
  11.9 15.1 %collective-permute-start.5 = (bf16[24,2048]{1,0:T(8,128)(2,1)S(1)}, bf16[24,2048]{1,0:T(8,128)(2,1)}, u32[]{:S(2)}, u32[]{:S(2)}) collective-permute-start(bf16[24,2048]{1,0:T(8,128)(2,1)S(1)} %get-tuple-element.45), channel_id=1, source_target_pairs={{0,160},{32,192},{64,224},{96,0},{128,32},{160,64},{192,96},{224,1... | collective-permute-start | bytes 294920 | tf_op jit(solution)/shard_map/ppermute | solution.py:26
  15.0 14.6 %collective-permute-start.2 = (bf16[24,2048]{1,0:T(8,128)(2,1)S(1)}, bf16[24,2048]{1,0:T(8,128)(2,1)S(1)}, u32[]{:S(2)}, u32[]{:S(2)}) collective-permute-start(bf16[24,2048]{1,0:T(8,128)(2,1)S(1)} %get-tuple-element.45), channel_id=1, source_target_pairs={{0,8},{8,16},{16,24},{24,0},{1,9},{9,17},{17,25},{25,1},{2,10},{10... | collective-permute-start | bytes 294920 | tf_op jit(solution)/shard_map/ppermute | solution.py:26
  16.5 15.0 %collective-permute-start.1 = (bf16[24,2048]{1,0:T(8,128)(2,1)S(1)}, bf16[24,2048]{1,0:T(8,128)(2,1)S(1)}, u32[]{:S(2)}, u32[]{:S(2)}) collective-permute-start(bf16[24,2048]{1,0:T(8,128)(2,1)S(1)} %get-tuple-element.45), channel_id=1, source_target_pairs={{0,16},{8,24},{16,0},{24,8},{1,17},{9,25},{17,1},{25,9},{2,18},{10... | collective-permute-start | bytes 294920 | tf_op jit(solution)/shard_map/ppermute | solution.py:26
  25.5 5.9 %collective-permute-start = (bf16[24,2048]{1,0:T(8,128)(2,1)S(1)}, bf16[24,2048]{1,0:T(8,128)(2,1)S(1)}, u32[]{:S(2)}, u32[]{:S(2)}) collective-permute-start(bf16[24,2048]{1,0:T(8,128)(2,1)S(1)} %get-tuple-element.45), channel_id=1, source_target_pairs={{0,24},{8,0},{16,8},{24,16},{1,25},{9,1},{17,9},{25,17},{2,26},{10... | collective-permute-start | bytes 294920 | tf_op jit(solution)/shard_map/ppermute | solution.py:26
  28.0 18.8 %collective-permute-start.10 = (bf16[72,2048]{1,0:T(8,128)(2,1)S(1)}, bf16[72,2048]{1,0:T(8,128)(2,1)S(1)}, u32[]{:S(2)}, u32[]{:S(2)}) collective-permute-start(bf16[72,2048]{1,0:T(8,128)(2,1)S(1)} %pad_maximum_fusion.1), channel_id=1, source_target_pairs={{0,8},{8,16},{16,24},{24,0},{1,9},{9,17},{17,25},{25,1},{2,10},{10... | collective-permute-start | bytes 884744 | tf_op jit(solution)/shard_map/ppermute | solution.py:26
  28.6 18.1 %collective-permute-start.9 = (bf16[72,2048]{1,0:T(8,128)(2,1)S(1)}, bf16[72,2048]{1,0:T(8,128)(2,1)S(1)}, u32[]{:S(2)}, u32[]{:S(2)}) collective-permute-start(bf16[72,2048]{1,0:T(8,128)(2,1)S(1)} %pad_maximum_fusion.1), channel_id=1, source_target_pairs={{0,16},{8,24},{16,0},{24,8},{1,17},{9,25},{17,1},{25,9},{2,18},{10... | collective-permute-start | bytes 884744 | tf_op jit(solution)/shard_map/ppermute | solution.py:26
  29.6 17.1 %collective-permute-start.8 = (bf16[72,2048]{1,0:T(8,128)(2,1)S(1)}, bf16[72,2048]{1,0:T(8,128)(2,1)S(1)}, u32[]{:S(2)}, u32[]{:S(2)}) collective-permute-start(bf16[72,2048]{1,0:T(8,128)(2,1)S(1)} %pad_maximum_fusion.1), channel_id=1, source_target_pairs={{0,24},{8,0},{16,8},{24,16},{1,25},{9,1},{17,9},{25,17},{2,26},{10... | collective-permute-start | bytes 884744 | tf_op jit(solution)/shard_map/ppermute | solution.py:26
  31.5 11.8 %collective-permute-start.4 = (bf16[96,2048]{1,0:T(8,128)(2,1)S(1)}, bf16[96,2048]{1,0:T(8,128)(2,1)S(1)}, u32[]{:S(2)}, u32[]{:S(2)}) collective-permute-start(bf16[96,2048]{1,0:T(8,128)(2,1)S(1)} %pad_maximum_fusion), channel_id=1, source_target_pairs={{0,32},{32,64},{64,96},{96,128},{128,160},{160,192},{192,224},{224... | collective-permute-start | bytes 1179656 | tf_op jit(solution)/shard_map/ppermute | solution.py:26
  33.7 9.5 %collective-permute-start.3 = (bf16[96,2048]{1,0:T(8,128)(2,1)S(1)}, bf16[96,2048]{1,0:T(8,128)(2,1)S(1)}, u32[]{:S(2)}, u32[]{:S(2)}) collective-permute-start(bf16[96,2048]{1,0:T(8,128)(2,1)S(1)} %pad_maximum_fusion), channel_id=1, source_target_pairs={{0,224},{32,0},{64,32},{96,64},{128,96},{160,128},{192,160},{224,1... | collective-permute-start | bytes 1179656 | tf_op jit(solution)/shard_map/ppermute | solution.py:26
  43.4 10.0 %collective-permute-start.12 = (bf16[96,2048]{1,0:T(8,128)(2,1)S(1)}, bf16[96,2048]{1,0:T(8,128)(2,1)S(1)}, u32[]{:S(2)}, u32[]{:S(2)}) collective-permute-start(bf16[96,2048]{1,0:T(8,128)(2,1)S(1)} %collective-permute-done.4), channel_id=1, source_target_pairs={{0,32},{32,64},{64,96},{96,128},{128,160},{160,192},{192,224},{224... | collective-permute-start | bytes 1179656 | tf_op jit(solution)/shard_map/ppermute | solution.py:26
  43.8 8.8 %collective-permute-start.11 = (bf16[96,2048]{1,0:T(8,128)(2,1)S(1)}, bf16[96,2048]{1,0:T(8,128)(2,1)S(1)}, u32[]{:S(2)}, u32[]{:S(2)}) collective-permute-start(bf16[96,2048]{1,0:T(8,128)(2,1)S(1)} %collective-permute-done.3), channel_id=1, source_target_pairs={{0,224},{32,0},{64,32},{96,64},{128,96},{160,128},{192,160},{224,1... | collective-permute-start | bytes 1179656 | tf_op jit(solution)/shard_map/ppermute | solution.py:26
  61.3 15.1 %all-to-all-start = ((f32[32,1,896]{2,1,0:T(1,128)}), f32[32,1,896]{2,1,0:T(1,128)S(1)}, u32[]{:S(2)}, u32[]{:S(2)}) async-start(f32[32,1,896]{2,1,0:T(1,128)} %broadcast_in_dim.16), calls=%async_computation | async-start | bytes 229376 | tf_op jit(solution)/shard_map/all_to_all | solution.py:185
  90.0 14.2 %collective-permute-start.17 = (bf16[72,2048]{1,0:T(8,128)(2,1)}, bf16[72,2048]{1,0:T(8,128)(2,1)}, u32[]{:S(2)}, u32[]{:S(2)}) collective-permute-start(bf16[72,2048]{1,0:T(8,128)(2,1)} %get-tuple-element.19), channel_id=1, source_target_pairs={{0,8},{8,16},{16,24},{24,0},{1,9},{9,17},{17,25},{25,1},{2,10},{10... | collective-permute-start | bytes 884744 | tf_op jit(solution)/shard_map/ppermute | solution.py:26
  90.2 14.1 %collective-permute-start.18 = (bf16[72,2048]{1,0:T(8,128)(2,1)}, bf16[72,2048]{1,0:T(8,128)(2,1)}, u32[]{:S(2)}, u32[]{:S(2)}) collective-permute-start(bf16[72,2048]{1,0:T(8,128)(2,1)} %get-tuple-element.20), channel_id=1, source_target_pairs={{0,16},{8,24},{16,0},{24,8},{1,17},{9,25},{17,1},{25,9},{2,18},{10... | collective-permute-start | bytes 884744 | tf_op jit(solution)/shard_map/ppermute | solution.py:26
  92.8 11.5 %collective-permute-start.19 = (bf16[72,2048]{1,0:T(8,128)(2,1)}, bf16[72,2048]{1,0:T(8,128)(2,1)}, u32[]{:S(2)}, u32[]{:S(2)}) collective-permute-start(bf16[72,2048]{1,0:T(8,128)(2,1)} %get-tuple-element.21), channel_id=1, source_target_pairs={{0,24},{8,0},{16,8},{24,16},{1,25},{9,1},{17,9},{25,17},{2,26},{10... | collective-permute-start | bytes 884744 | tf_op jit(solution)/shard_map/ppermute | solution.py:26
  94.5 11.1 %collective-permute-start.13 = (bf16[96,2048]{1,0:T(8,128)(2,1)}, bf16[96,2048]{1,0:T(8,128)(2,1)S(1)}, u32[]{:S(2)}, u32[]{:S(2)}) collective-permute-start(bf16[96,2048]{1,0:T(8,128)(2,1)} %get-tuple-element.16), channel_id=1, source_target_pairs={{0,32},{32,64},{64,96},{96,128},{128,160},{160,192},{192,224},{224... | collective-permute-start | bytes 1179656 | tf_op jit(solution)/shard_map/ppermute | solution.py:26
  95.1 10.5 %collective-permute-start.15 = (bf16[96,2048]{1,0:T(8,128)(2,1)}, bf16[96,2048]{1,0:T(8,128)(2,1)}, u32[]{:S(2)}, u32[]{:S(2)}) collective-permute-start(bf16[96,2048]{1,0:T(8,128)(2,1)} %get-tuple-element.17), channel_id=1, source_target_pairs={{0,224},{32,0},{64,32},{96,64},{128,96},{160,128},{192,160},{224,1... | collective-permute-start | bytes 1179656 | tf_op jit(solution)/shard_map/ppermute | solution.py:26
  104.2 32.3 %collective-permute-start.26 = (bf16[1024,1024]{1,0:T(8,128)(2,1)}, bf16[1024,1024]{1,0:T(8,128)(2,1)}, u32[]{:S(2)}, u32[]{:S(2)}) collective-permute-start(bf16[1024,1024]{1,0:T(8,128)(2,1)} %shard_map.113), channel_id=1, source_target_pairs={{0,1},{1,0},{2,3},{3,2},{4,5},{5,4},{6,7},{7,6},{8,9},{9,8},{10,11... | collective-permute-start | bytes 6291464 | tf_op jit(solution)/shard_map/ppermute | solution.py:26
  105.6 30.6 %copy-start.4 = (bf16[24,1,2048]{2,0,1:T(8,128)(2,1)S(1)}, bf16[24,1,2048]{2,0,1:T(8,128)(2,1)}, u32[]{:S(2)}) copy-start(bf16[24,1,2048]{2,0,1:T(8,128)(2,1)} %param.9) | copy-start | bytes 294916
  106.9 19.5 %collective-permute-start.14 = (bf16[96,2048]{1,0:T(8,128)(2,1)S(1)}, bf16[96,2048]{1,0:T(8,128)(2,1)S(1)}, u32[]{:S(2)}, u32[]{:S(2)}) collective-permute-start(bf16[96,2048]{1,0:T(8,128)(2,1)S(1)} %get-tuple-element.46), channel_id=1, source_target_pairs={{0,32},{32,64},{64,96},{96,128},{128,160},{160,192},{192,224},{224... | collective-permute-start | bytes 1179656 | tf_op jit(solution)/shard_map/ppermute | solution.py:26
  107.2 19.2 %collective-permute-start.16 = (bf16[96,2048]{1,0:T(8,128)(2,1)S(1)}, bf16[96,2048]{1,0:T(8,128)(2,1)S(1)}, u32[]{:S(2)}, u32[]{:S(2)}) collective-permute-start(bf16[96,2048]{1,0:T(8,128)(2,1)S(1)} %get-tuple-element.47), channel_id=1, source_target_pairs={{0,224},{32,0},{64,32},{96,64},{128,96},{160,128},{192,160},{224,1... | collective-permute-start | bytes 1179656 | tf_op jit(solution)/shard_map/ppermute | solution.py:26
  110.4 18.5 %collective-permute-start.20 = (bf16[24,2048]{1,0:T(8,128)(2,1)S(1)}, bf16[24,2048]{1,0:T(8,128)(2,1)S(1)}, u32[]{:S(2)}, u32[]{:S(2)}) collective-permute-start(bf16[24,2048]{1,0:T(8,128)(2,1)S(1)} %get-tuple-element.51), channel_id=1, source_target_pairs={{0,128},{32,160},{64,192},{96,224},{128,0},{160,32},{192,64},{224,... | collective-permute-start | bytes 294920 | tf_op jit(solution)/shard_map/ppermute | solution.py:26
  111.6 18.7 %collective-permute-start.22 = (bf16[24,2048]{1,0:T(8,128)(2,1)S(1)}, bf16[24,2048]{1,0:T(8,128)(2,1)S(1)}, u32[]{:S(2)}, u32[]{:S(2)}) collective-permute-start(bf16[24,2048]{1,0:T(8,128)(2,1)S(1)} %get-tuple-element.52), channel_id=1, source_target_pairs={{0,160},{32,192},{64,224},{96,0},{128,32},{160,64},{192,96},{224,1... | collective-permute-start | bytes 294920 | tf_op jit(solution)/shard_map/ppermute | solution.py:26
  126.4 7.6 %collective-permute-start.21 = (bf16[24,2048]{1,0:T(8,128)(2,1)S(1)}, bf16[24,2048]{1,0:T(8,128)(2,1)S(1)}, u32[]{:S(2)}, u32[]{:S(2)}) collective-permute-start(bf16[24,2048]{1,0:T(8,128)(2,1)S(1)} %get-tuple-element.53), channel_id=1, source_target_pairs={{0,96},{32,128},{64,160},{96,192},{128,224},{160,0},{192,32},{224,... | collective-permute-start | bytes 294920 | tf_op jit(solution)/shard_map/ppermute | solution.py:26
  126.5 7.5 %collective-permute-start.23 = (bf16[24,2048]{1,0:T(8,128)(2,1)S(1)}, bf16[24,2048]{1,0:T(8,128)(2,1)S(1)}, u32[]{:S(2)}, u32[]{:S(2)}) collective-permute-start(bf16[24,2048]{1,0:T(8,128)(2,1)S(1)} %get-tuple-element.48), channel_id=1, source_target_pairs={{0,16},{8,24},{16,0},{24,8},{1,17},{9,25},{17,1},{25,9},{2,18},{10... | collective-permute-start | bytes 294920 | tf_op jit(solution)/shard_map/ppermute | solution.py:26
  128.9 5.1 %collective-permute-start.25 = (bf16[24,2048]{1,0:T(8,128)(2,1)S(1)}, bf16[24,2048]{1,0:T(8,128)(2,1)S(1)}, u32[]{:S(2)}, u32[]{:S(2)}) collective-permute-start(bf16[24,2048]{1,0:T(8,128)(2,1)S(1)} %get-tuple-element.49), channel_id=1, source_target_pairs={{0,24},{8,0},{16,8},{24,16},{1,25},{9,1},{17,9},{25,17},{2,26},{10... | collective-permute-start | bytes 294920 | tf_op jit(solution)/shard_map/ppermute | solution.py:26
  130.4 5.8 %collective-permute-start.24 = (bf16[24,2048]{1,0:T(8,128)(2,1)S(1)}, bf16[24,2048]{1,0:T(8,128)(2,1)S(1)}, u32[]{:S(2)}, u32[]{:S(2)}) collective-permute-start(bf16[24,2048]{1,0:T(8,128)(2,1)S(1)} %get-tuple-element.50), channel_id=1, source_target_pairs={{0,8},{8,16},{16,24},{24,0},{1,9},{9,17},{17,25},{25,1},{2,10},{10... | collective-permute-start | bytes 294920 | tf_op jit(solution)/shard_map/ppermute | solution.py:26
  142.1 16.5 %collective-permute-start.27 = (bf16[256,1024]{1,0:T(8,128)(2,1)}, bf16[256,1024]{1,0:T(8,128)(2,1)S(1)}, u32[]{:S(2)}, u32[]{:S(2)}) collective-permute-start(bf16[256,1024]{1,0:T(8,128)(2,1)} %get-tuple-element.24), channel_id=1, source_target_pairs={{0,4},{2,6},{4,0},{6,2},{1,5},{3,7},{5,1},{7,3},{8,12},{10,14},{12... | collective-permute-start | bytes 1572872 | tf_op jit(solution)/shard_map/ppermute | solution.py:26
  144.5 22.6 %collective-permute-start.28 = (bf16[256,1024]{1,0:T(8,128)(2,1)}, bf16[256,1024]{1,0:T(8,128)(2,1)S(1)}, u32[]{:S(2)}, u32[]{:S(2)}) collective-permute-start(bf16[256,1024]{1,0:T(8,128)(2,1)} %get-tuple-element.25), channel_id=1, source_target_pairs={{0,2},{2,4},{4,6},{6,0},{1,3},{3,5},{5,7},{7,1},{8,10},{10,12},{12... | collective-permute-start | bytes 1572872 | tf_op jit(solution)/shard_map/ppermute | solution.py:26
  144.5 22.6 %collective-permute-start.29 = (bf16[256,1024]{1,0:T(8,128)(2,1)}, bf16[256,1024]{1,0:T(8,128)(2,1)S(1)}, u32[]{:S(2)}, u32[]{:S(2)}) collective-permute-start(bf16[256,1024]{1,0:T(8,128)(2,1)} %get-tuple-element.26), channel_id=1, source_target_pairs={{0,6},{2,0},{4,2},{6,4},{1,7},{3,1},{5,3},{7,5},{8,14},{10,8},{12,... | collective-permute-start | bytes 1572872 | tf_op jit(solution)/shard_map/ppermute | solution.py:26
  (11 other events, 170.6 us)
where the time goes:
time: 171 us; the launch traced here: 170 us
  waiting for transfers between devices  62 us (36%)
  starting transfers between devices  55.7 us (33%)
  Pallas kernels  24.9 us (15%)
  other arithmetic  16 us (9%)
  matrix products  5.33 us (3%)
  local copies, waits for them, and re-layouts  4.54 us (3%)
    ppermute x30, waiting for transfers between devices, taken_from(): lax.ppermute(array, axis, [(i, (i - step) % count) for i in range(count)])  51.6 us
    ppermute x30, starting transfers between devices, taken_from(): lax.ppermute(array, axis, [(i, (i - step) % count) for i in range(count)])  51 us
    pallas_call x1, Pallas kernels, whole(): pl.pallas_call(gradient_kernel, out_shape=shaped(((total_rows, columns),...  12.8 us
    all_to_all x1, waiting for transfers between devices, whole(): lax.all_to_all(packed, VP, split_axis=0, concat_axis=0, tiled=True)[:, 0]  10.3 us
    pallas_call x1, Pallas kernels, whole(): pl.pallas_call(other_kernel, out_shape=shaped(((NY * share, columns), bf1...  6.4 us
    pallas_call x1, Pallas kernels, whole(): pl.pallas_call(chip_kernel, out_shape=shaped(((share, columns), f32), *[(...  5.7 us
    all_to_all x1, starting transfers between devices, whole(): lax.all_to_all(packed, VP, split_axis=0, concat_axis=0, tiled=True)[:, 0]  4.7 us
    dot_general x1, matrix products, whole(): jnp.dot(rows_all, vocab_matrix, preferred_element_type=f32)  3.55 us
  transfers between devices with their start and end apart: 31, of which 9 were waited for; matrix products, arithmetic and copies ran while one was open for 7% of the time, Pallas kernels for 4%

commit v1 on v0

--- a/solution.py
+++ b/solution.py
@@ -55,85 +55,133 @@
     left = vectors - high.astype(f32)
     middle = left.astype(bf16)
     low = (left - middle.astype(f32)).astype(bf16)
-    return sum(
-        lax.dot_general(order, part, (((1,), (1,)), ((), ())), preferred_element_type=f32)
-        for part in (high, middle, low)
-    )
+    count = vectors.shape[0]
+    parts = jnp.concatenate([high.astype(f32), middle.astype(f32), low.astype(f32)])
+    moved_parts = lax.dot_general(
+        order, parts.astype(bf16), (((1,), (1,)), ((), ())), preferred_element_type=f32
+    )
+    return [
+        sum(moved_parts[:, k + count * part : k + count * part + 1] for part in range(3))
+        for k in range(3)
+    ]
 
 
 def gradient_kernel(
     scores, matrix, order, vectors, grad, far_own, near, upward, downward, *far_away
 ):
-    columns = column_vectors(order[...], vectors[...])
-    log_total, weights, target = columns[:, 0:1], columns[:, 1:2], columns[:, 2:3]
-    scale = weights * (1.0 + 2.0 * penalty * log_total)
-    target = target.astype(jnp.int32)
-    rows, width = scores.shape
-    step = 256
-    for low in range(0, width, step):
-        part = slice(low, low + step)
-        ids = lax.broadcasted_iota(jnp.int32, (rows, step), 1) + low
-        probs = jnp.exp(scores[:, part] - log_total)
-        grad[:, part] = (
-            scale * probs - jnp.where(ids == target, weights, 0.0)
-        ).astype(bf16)
+    @pl.when(pl.program_id(0) == 0)
+    def first():
+        log_total, weights, target = column_vectors(order[...], vectors[...])
+        scale = weights * (1.0 + 2.0 * penalty * log_total)
+        target = target.astype(jnp.int32)
+        rows, width = scores.shape
+        step = 128
+        for low in range(0, width, step):
+            part = slice(low, low + step)
+            ids = lax.broadcasted_iota(jnp.int32, (rows, step), 1) + low
+            probs = jnp.exp(scores[:, part] - log_total)
+            grad[:, part] = (
+                scale * probs - jnp.where(ids == target, weights, 0.0)
+            ).astype(bf16)
 
     block, wide = upward.shape[0], far_own.shape[0]
-
-    def body(number, carry):
-        part = pl.ds(pl.multiple_of(number * step, step), step)
-        out = lax.dot_general(
-            grad[...], matrix[part, :], (((1,), (1,)), ((), ())), preferred_element_type=f32
-        )
-        near[:, part] = out[: 3 * block]
-        at = 3 * block
-        far_own[:, part] = out[at : at + wide]
-        for ref in far_away:
-            at += wide
-            ref[:, part] = out[at : at + wide].astype(bf16)
+    out = lax.dot_general(
+        grad[...], matrix[...], (((1,), (1,)), ((), ())), preferred_element_type=f32
+    )
+    near[...] = out[: 3 * block]
+    at = 3 * block
+    far_own[...] = out[at : at + wide]
+    for ref in far_away:
         at += wide
-        upward[:, part] = out[at : at + block].astype(bf16)
-        downward[:, part] = out[at + block :].astype(bf16)
-        return carry
-
-    lax.fori_loop(0, matrix.shape[0] // step, body, 0)
-
-
-def vocab_product(rows, grad, first, share):
-    part = pl.ds(pl.multiple_of(first * share, share), share)
+        ref[...] = out[at : at + wide].astype(bf16)
+    at += wide
+    upward[...] = out[at : at + block].astype(bf16)
+    downward[...] = out[at + block :].astype(bf16)
+
+
+def gradients(scores, matrix, order, vectors, block, wide):
+    rows, columns = scores.shape
+    width = matrix.shape[0]
+    step = 512
+    kinds = [(wide, f32), (3 * block, f32), (block, bf16), (block, bf16)]
+    kinds += [(wide, bf16)] * (NX - 1)
+    return pl.pallas_call(
+        gradient_kernel,
+        grid=(width // step,),
+        out_shape=[jax.ShapeDtypeStruct((rows, columns), bf16)]
+        + [jax.ShapeDtypeStruct((count, width), kind) for count, kind in kinds],
+        in_specs=[
+            pl.BlockSpec(scores.shape, lambda i: (0, 0)),
+            pl.BlockSpec((step, columns), lambda i: (i, 0)),
+            pl.BlockSpec(order.shape, lambda i: (0, 0)),
+            pl.BlockSpec(vectors.shape, lambda i: (0, 0)),
+        ],
+        out_specs=[pl.BlockSpec((rows, columns), lambda i: (0, 0))]
+        + [pl.BlockSpec((count, step), lambda i: (0, i)) for count, kind in kinds],
+    )(scores, matrix, order, vectors)
+
+
+def product_over_tokens(rows, grad):
     return lax.dot_general(
-        rows[:, part], grad[...], (((0,), (0,)), ((), ())), preferred_element_type=f32
+        rows[...], grad[...], (((0,), (0,)), ((), ())), preferred_element_type=f32
     )
 
 
 def other_kernel(place, rows, grad, out):
+    out[...] = product_over_tokens(rows, grad).astype(bf16)
+
+
+def chip_kernel(place, rows, grad, other, own, *away):
+    product = product_over_tokens(rows, grad) + other[...].astype(f32)
+    for k, ref in enumerate((own, *away)):
+
+        @pl.when(pl.program_id(0) == NY - 1 - k)
+        def store(ref=ref):
+            ref[...] = product.astype(ref.dtype)
+
+
+def other_product(place, rows, grad):
     share = rows.shape[1] // (NY * NC)
-
-    def body(y, carry):
-        product = vocab_product(rows, grad, y * NC + 1 - place[1], share)
-        out[pl.ds(pl.multiple_of(y * share, share), share), :] = product.astype(bf16)
-        return carry
-
-    lax.fori_loop(0, NY, body, 0)
-
-
-def chip_kernel(place, rows, grad, other, own, *away):
+    tokens, columns = grad.shape
+    return pl.pallas_call(
+        other_kernel,
+        out_shape=jax.ShapeDtypeStruct((NY * share, columns), bf16),
+        grid_spec=pltpu.PrefetchScalarGridSpec(
+            num_scalar_prefetch=1,
+            grid=(NY,),
+            in_specs=[
+                pl.BlockSpec((tokens, share), lambda y, place: (0, y * NC + 1 - place[1])),
+                pl.BlockSpec((tokens, columns), lambda y, place: (0, 0)),
+            ],
+            out_specs=pl.BlockSpec((share, columns), lambda y, place: (y, 0)),
+        ),
+    )(place, rows, grad)
+
+
+def chip_products(place, rows, grad, other):
     share = rows.shape[1] // (NY * NC)
-    for k, ref in enumerate((own, *away)):
-        y = lax.rem(place[0] + k, NY)
-        product = vocab_product(rows, grad, y * NC + place[1], share)
-        product = product + other[pl.ds(pl.multiple_of(y * share, share), share), :].astype(f32)
-        ref[...] = product.astype(ref.dtype)
-
-
-def shaped(*shapes):
-    return tuple(jax.ShapeDtypeStruct(dims, kind) for dims, kind in shapes)
-
-
-def spaces(scalars, arrays):
-    return [pl.BlockSpec(memory_space=pltpu.SMEM)] * scalars + [
-        pl.BlockSpec(memory_space=pltpu.VMEM)
-    ] * arrays
+    tokens, columns = grad.shape
+
+    def at(step, place):
+        return lax.rem(place[0] + NY - 1 - step, NY)
+
+    return pl.pallas_call(
+        chip_kernel,
+        out_shape=[jax.ShapeDtypeStruct((share, columns), f32)]
+        + [jax.ShapeDtypeStruct((share, columns), bf16)] * (NY - 1),
+        grid_spec=pltpu.PrefetchScalarGridSpec(
+            num_scalar_prefetch=1,
+            grid=(NY,),
+            in_specs=[
+                pl.BlockSpec(
+                    (tokens, share), lambda step, place: (0, at(step, place) * NC + place[1])
+                ),
+                pl.BlockSpec((tokens, columns), lambda step, place: (0, 0)),
+                pl.BlockSpec((share, columns), lambda step, place: (at(step, place), 0)),
+            ],
+            out_specs=[pl.BlockSpec((share, columns), lambda step, place: (0, 0))] * NY,
+        ),
+    )(place, rows, grad, other)
 
 
 def whole(hidden_rows, norm_gain, vocab_matrix, vocab_bias, targets, loss_weight):
@@ -141,7 +189,7 @@
     inverse_rms = lax.rsqrt(jnp.mean(inputs * inputs, axis=-1, keepdims=True) + epsilon)
     unit_rows = inputs * inverse_rms
     normed = (unit_rows * norm_gain).astype(bf16)
-    own, width = normed.shape
+    own, _ = normed.shape
     total_rows = own * NZ * NX
     columns = vocab_matrix.shape[1]
 
@@ -200,40 +248,17 @@
     )
     block = NX * own
     wide = len(FAR) * own
-    score_grad, far_own, near, upward, downward, *far_away = pl.pallas_call(
-        gradient_kernel,
-        out_shape=shaped(
-            ((total_rows, columns), bf16),
-            ((wide, width), f32),
-            ((3 * block, width), f32),
-            ((block, width), bf16),
-            ((block, width), bf16),
-            *[((wide, width), bf16)] * (NX - 1),
-        ),
-        in_specs=spaces(0, 4),
-        out_specs=spaces(0, 5 + NX - 1),
-    )(scores, vocab_matrix, order, vectors)
+    score_grad, far_own, near, upward, downward, *far_away = gradients(
+        scores, vocab_matrix, order, vectors, block, wide
+    )
     from_below = sent_to(upward, "vp_0", 1)
     from_above = sent_to(downward, "vp_0", -1)
     far_x = {kx: sent_to(far_away[kx - 1], "vp_1", kx) for kx in (2, 1, 3)}
 
-    share = width // (NY * NC)
     place = jnp.stack([lax.axis_index("dp_0"), lax.axis_index("dp_1")])
-    (other,) = pl.pallas_call(
-        other_kernel,
-        out_shape=shaped(((NY * share, columns), bf16)),
-        in_specs=spaces(1, 2),
-        out_specs=spaces(0, 1),
-    )(place, rows_all, score_grad)
+    other = other_product(place, rows_all, score_grad)
     other = taken_from(other, "dp_1", 1)
-    vocab_grad, *away = pl.pallas_call(
-        chip_kernel,
-        out_shape=shaped(
-            ((share, columns), f32), *[((share, columns), bf16)] * (NY - 1)
-        ),
-        in_specs=spaces(1, 3),
-        out_specs=spaces(0, NY),
-    )(place, rows_all, score_grad, other)
+    vocab_grad, *away = chip_products(place, rows_all, score_grad, other)
     chip_y = {k: sent_to(away[k - 1], "dp_0", k) for k in (2, 1, 3)}
     above, below = near[block : 2 * block], near[2 * block :]
     from_below = sent_to((above + from_below.astype(f32)).astype(bf16), "vp_0", 1)

time: 171 us -> 170 us (level)
  transfers between devices with their start and end apart: 31 -> 31, of which waited for: 9 -> 9; matrix products, arithmetic and copies ran while one was open for 7% -> 8% of each run, Pallas kernels for 4% -> 4%
where the time goes in v1:
time: 170 us; the launch traced here: 169 us
  waiting for transfers between devices  62.1 us (37%)
  starting transfers between devices  55.7 us (33%)
  Pallas kernels  23.8 us (14%)
  other arithmetic  16 us (9%)
  matrix products  5.33 us (3%)
  local copies, waits for them, and re-layouts  4.54 us (3%)
    ppermute x30, waiting for transfers between devices, taken_from(): lax.ppermute(array, axis, [(i, (i - step) % count) for i in range(count)])  51.8 us
    ppermute x30, starting transfers between devices, taken_from(): lax.ppermute(array, axis, [(i, (i - step) % count) for i in range(count)])  51 us
    all_to_all x1, waiting for transfers between devices, whole(): lax.all_to_all(packed, VP, split_axis=0, concat_axis=0, tiled=True)[:, 0]  10.3 us
    pallas_call x1, Pallas kernels, gradients(): pl.pallas_call(gradient_kernel, grid=(width // step,), out_shape=[jax.Sha...  10.3 us
    pallas_call x1, Pallas kernels, chip_products(): pl.pallas_call(chip_kernel, out_shape=[jax.ShapeDtypeStruct((share, colum...  7.2 us
    pallas_call x1, Pallas kernels, other_product(): pl.pallas_call(other_kernel, out_shape=jax.ShapeDtypeStruct((NY * share,...  6.3 us
    all_to_all x1, starting transfers between devices, whole(): lax.all_to_all(packed, VP, split_axis=0, concat_axis=0, tiled=True)[:, 0]  4.7 us
    dot_general x1, matrix products, whole(): jnp.dot(rows_all, vocab_matrix, preferred_element_type=f32)  3.55 us
  transfers between devices with their start and end apart: 31, of which 9 were waited for; matrix products, arithmetic and copies ran while one was open for 8% of the time, Pallas kernels for 4%

profile of v1, /device:TPU:8, one launch (start us, length us, event | category | flops | bytes accessed | tf_op | source)
XLA Modules:
  0.0 168.6 jit_solution(2812379814648782807)
XLA Ops:
  2.7 4.7 %collective-permute-start.7 = (bf16[24,2048]{1,0:T(8,128)(2,1)S(1)}, bf16[24,2048]{1,0:T(8,128)(2,1)S(1)}, u32[]{:S(2)}, u32[]{:S(2)}) collective-permute-start(bf16[24,2048]{1,0:T(8,128)(2,1)S(1)} %get-tuple-element.45), channel_id=1, source_target_pairs={{0,96},{32,128},{64,160},{96,192},{128,224},{160,0},{192,32},{224,... | collective-permute-start | bytes 294920 | tf_op jit(solution)/shard_map/ppermute | solution.py:26
  7.4 4.5 %collective-permute-start.6 = (bf16[24,2048]{1,0:T(8,128)(2,1)S(1)}, bf16[24,2048]{1,0:T(8,128)(2,1)}, u32[]{:S(2)}, u32[]{:S(2)}) collective-permute-start(bf16[24,2048]{1,0:T(8,128)(2,1)S(1)} %get-tuple-element.45), channel_id=1, source_target_pairs={{0,128},{32,160},{64,192},{96,224},{128,0},{160,32},{192,64},{224,... | collective-permute-start | bytes 294920 | tf_op jit(solution)/shard_map/ppermute | solution.py:26
  11.9 3.1 %collective-permute-start.5 = (bf16[24,2048]{1,0:T(8,128)(2,1)S(1)}, bf16[24,2048]{1,0:T(8,128)(2,1)}, u32[]{:S(2)}, u32[]{:S(2)}) collective-permute-start(bf16[24,2048]{1,0:T(8,128)(2,1)S(1)} %get-tuple-element.45), channel_id=1, source_target_pairs={{0,160},{32,192},{64,224},{96,0},{128,32},{160,64},{192,96},{224,1... | collective-permute-start | bytes 294920 | tf_op jit(solution)/shard_map/ppermute | solution.py:26
  15.0 1.5 collective-permute-start.2
  16.5 2.7 %collective-permute-start.1 = (bf16[24,2048]{1,0:T(8,128)(2,1)S(1)}, bf16[24,2048]{1,0:T(8,128)(2,1)S(1)}, u32[]{:S(2)}, u32[]{:S(2)}) collective-permute-start(bf16[24,2048]{1,0:T(8,128)(2,1)S(1)} %get-tuple-element.45), channel_id=1, source_target_pairs={{0,16},{8,24},{16,0},{24,8},{1,17},{9,25},{17,1},{25,9},{2,18},{10... | collective-permute-start | bytes 294920 | tf_op jit(solution)/shard_map/ppermute | solution.py:26
  25.5 1.5 collective-permute-start
  29.6 1.9 %collective-permute-start.8 = (bf16[72,2048]{1,0:T(8,128)(2,1)S(1)}, bf16[72,2048]{1,0:T(8,128)(2,1)S(1)}, u32[]{:S(2)}, u32[]{:S(2)}) collective-permute-start(bf16[72,2048]{1,0:T(8,128)(2,1)S(1)} %pad_maximum_fusion.1), channel_id=1, source_target_pairs={{0,24},{8,0},{16,8},{24,16},{1,25},{9,1},{17,9},{25,17},{2,26},{10... | collective-permute-start | bytes 884744 | tf_op jit(solution)/shard_map/ppermute | solution.py:26
  31.5 2.2 %collective-permute-start.4 = (bf16[96,2048]{1,0:T(8,128)(2,1)S(1)}, bf16[96,2048]{1,0:T(8,128)(2,1)S(1)}, u32[]{:S(2)}, u32[]{:S(2)}) collective-permute-start(bf16[96,2048]{1,0:T(8,128)(2,1)S(1)} %pad_maximum_fusion), channel_id=1, source_target_pairs={{0,32},{32,64},{64,96},{96,128},{128,160},{160,192},{192,224},{224... | collective-permute-start | bytes 1179656 | tf_op jit(solution)/shard_map/ppermute | solution.py:26
  34.8 8.4 %collective-permute-done.3 = bf16[96,2048]{1,0:T(8,128)(2,1)S(1)} collective-permute-done((bf16[96,2048]{1,0:T(8,128)(2,1)S(1)}, bf16[96,2048]{1,0:T(8,128)(2,1)S(1)}, u32[]{:S(2)}, u32[]{:S(2)}) %collective-permute-start.3) | collective-permute-done | bytes 393248 | tf_op jit(solution)/shard_map/ppermute | solution.py:26
  43.8 2.9 %collective-permute-start.11 = (bf16[96,2048]{1,0:T(8,128)(2,1)S(1)}, bf16[96,2048]{1,0:T(8,128)(2,1)S(1)}, u32[]{:S(2)}, u32[]{:S(2)}) collective-permute-start(bf16[96,2048]{1,0:T(8,128)(2,1)S(1)} %collective-permute-done.3), channel_id=1, source_target_pairs={{0,224},{32,0},{64,32},{96,64},{128,96},{160,128},{192,160},{224,1... | collective-permute-start | bytes 1179656 | tf_op jit(solution)/shard_map/ppermute | solution.py:26
  46.8 5.8 %collective-permute-done.11 = bf16[96,2048]{1,0:T(8,128)(2,1)S(1)} collective-permute-done((bf16[96,2048]{1,0:T(8,128)(2,1)S(1)}, bf16[96,2048]{1,0:T(8,128)(2,1)S(1)}, u32[]{:S(2)}, u32[]{:S(2)}) %collective-permute-start.11) | collective-permute-done | bytes 393248 | tf_op jit(solution)/shard_map/ppermute | solution.py:26
  53.4 3.6 %fusion.42 = (f32[768]{0:T(1024)S(1)}, f32[768,1024]{1,0:T(8,128)S(1)}) fusion(f32[1024]{0:T(1024)S(1)} %copy-done.11, bf16[768,2048]{1,0:T(8,128)(2,1)S(1)} %constant_dynamic-update-slice_fusion.rows, bf16[2048,1024]{1,0:T(8,128)(2,1)S(1)} %copy-done.2), kind=kOutput, calls=%fused_computation.113 | convolution fusion | flops 3222797568 | bytes 10492928 | tf_op jit(solution)/shard_map/dot_general | solution.py:223
  57.0 1.6 copy-done.1
  61.3 4.7 %all-to-all-start = ((f32[32,1,896]{2,1,0:T(1,128)}), f32[32,1,896]{2,1,0:T(1,128)S(1)}, u32[]{:S(2)}, u32[]{:S(2)}) async-start(f32[32,1,896]{2,1,0:T(1,128)} %broadcast_in_dim.16), calls=%async_computation | async-start | bytes 229376 | tf_op jit(solution)/shard_map/all_to_all | solution.py:233
  66.0 10.3 %all-to-all-done = f32[32,1,896]{2,1,0:T(1,128)S(1)} async-done(((f32[32,1,896]{2,1,0:T(1,128)}), f32[32,1,896]{2,1,0:T(1,128)S(1)}, u32[]{:S(2)}, u32[]{:S(2)}) %all-to-all-start) | async-done | bytes 114720 | tf_op jit(solution)/shard_map/all_to_all | solution.py:233
  77.1 10.3 %shard_map.112 = (bf16[768,1024]{1,0:T(8,128)(2,1)}, f32[72,2048]{1,0:T(8,128)}, f32[288,2048]{1,0:T(8,128)}, bf16[96,2048]{1,0:T(8,128)(2,1)}, bf16[96,2048]{1,...) custom-call(f32[768,1024]{1,0:T(8,128)} %copy-done.1, ...), custom_call_target="tpu_custom_call" | custom-call | tf_op jit(solution)/shard_map/pallas_call | solution.py:108
  87.8 2.6 %collective-permute-start.18 = (bf16[72,2048]{1,0:T(8,128)(2,1)}, bf16[72,2048]{1,0:T(8,128)(2,1)}, u32[]{:S(2)}, u32[]{:S(2)}) collective-permute-start(bf16[72,2048]{1,0:T(8,128)(2,1)} %get-tuple-element.20), channel_id=1, source_target_pairs={{0,16},{8,24},{16,0},{24,8},{1,17},{9,25},{17,1},{25,9},{2,18},{10... | collective-permute-start | bytes 884744 | tf_op jit(solution)/shard_map/ppermute | solution.py:26
  92.7 2.6 %collective-permute-start.15 = (bf16[96,2048]{1,0:T(8,128)(2,1)}, bf16[96,2048]{1,0:T(8,128)(2,1)}, u32[]{:S(2)}, u32[]{:S(2)}) collective-permute-start(bf16[96,2048]{1,0:T(8,128)(2,1)} %get-tuple-element.17), channel_id=1, source_target_pairs={{0,224},{32,0},{64,32},{96,64},{128,96},{160,128},{192,160},{224,1... | collective-permute-start | bytes 1179656 | tf_op jit(solution)/shard_map/ppermute | solution.py:26
  95.3 6.3 %shard_map.113 = bf16[1024,1024]{1,0:T(8,128)(2,1)} custom-call(s32[2]{0:T(128)} %pad_add_fusion.place, bf16[768,2048]{1,0:T(8,128)(2,1)} %copy-done, bf16[768,1024]{1,0:T(8,128)(2,1)} %get-tuple-element.22.grad), custom_call_target="tpu_custom_call" | custom-call | tf_op jit(solution)/shard_map/pallas_call | solution.py:146
  104.7 3.2 %collective-permute-start.16 = (bf16[96,2048]{1,0:T(8,128)(2,1)S(1)}, bf16[96,2048]{1,0:T(8,128)(2,1)S(1)}, u32[]{:S(2)}, u32[]{:S(2)}) collective-permute-start(bf16[96,2048]{1,0:T(8,128)(2,1)S(1)} %get-tuple-element.47), channel_id=1, source_target_pairs={{0,224},{32,0},{64,32},{96,64},{128,96},{160,128},{192,160},{224,1... | collective-permute-start | bytes 1179656 | tf_op jit(solution)/shard_map/ppermute | solution.py:26
  109.1 2.2 %collective-permute-start.22 = (bf16[24,2048]{1,0:T(8,128)(2,1)S(1)}, bf16[24,2048]{1,0:T(8,128)(2,1)S(1)}, u32[]{:S(2)}, u32[]{:S(2)}) collective-permute-start(bf16[24,2048]{1,0:T(8,128)(2,1)S(1)} %get-tuple-element.52), channel_id=1, source_target_pairs={{0,160},{32,192},{64,224},{96,0},{128,32},{160,64},{192,96},{224,1... | collective-permute-start | bytes 294920 | tf_op jit(solution)/shard_map/ppermute | solution.py:26
  111.3 12.6 %collective-permute-done.14 = bf16[96,2048]{1,0:T(8,128)(2,1)S(1)} collective-permute-done((bf16[96,2048]{1,0:T(8,128)(2,1)S(1)}, bf16[96,2048]{1,0:T(8,128)(2,1)S(1)}, u32[]{:S(2)}, u32[]{:S(2)}) %collective-permute-start.14) | collective-permute-done | bytes 393248 | tf_op jit(solution)/shard_map/ppermute | solution.py:26
  124.1 2.4 %collective-permute-start.23 = (bf16[24,2048]{1,0:T(8,128)(2,1)S(1)}, bf16[24,2048]{1,0:T(8,128)(2,1)S(1)}, u32[]{:S(2)}, u32[]{:S(2)}) collective-permute-start(bf16[24,2048]{1,0:T(8,128)(2,1)S(1)} %get-tuple-element.48), channel_id=1, source_target_pairs={{0,16},{8,24},{16,0},{24,8},{1,17},{9,25},{17,1},{25,9},{2,18},{10... | collective-permute-start | bytes 294920 | tf_op jit(solution)/shard_map/ppermute | solution.py:26
  126.5 1.5 collective-permute-start.25
  129.1 2.5 %collective-permute-done.21 = bf16[24,2048]{1,0:T(8,128)(2,1)S(1)} collective-permute-done((bf16[24,2048]{1,0:T(8,128)(2,1)S(1)}, bf16[24,2048]{1,0:T(8,128)(2,1)S(1)}, u32[]{:S(2)}, u32[]{:S(2)}) %collective-permute-start.21) | collective-permute-done | bytes 98336 | tf_op jit(solution)/shard_map/ppermute | solution.py:26
  131.6 2.2 %collective-permute-done.24 = bf16[24,2048]{1,0:T(8,128)(2,1)S(1)} collective-permute-done((bf16[24,2048]{1,0:T(8,128)(2,1)S(1)}, bf16[24,2048]{1,0:T(8,128)(2,1)S(1)}, u32[]{:S(2)}, u32[]{:S(2)}) %collective-permute-start.24) | collective-permute-done | bytes 98336 | tf_op jit(solution)/shard_map/ppermute | solution.py:26
  134.0 7.2 %shard_map.114 = (f32[256,1024]{1,0:T(8,128)}, bf16[256,1024]{1,0:T(8,128)(2,1)}, bf16[256,1024]{1,0:T(8,128)(2,1)}, bf16[256,1024]{1,0:T(8,128)(2,1)}) custom-call(s32[2]{0:T(128)} %pad_add_fusion.place, bf16[768,2048]{1,0:T(8,128)(2,1)} %copy-done, bf16[768,1024]{1,0:T(8,128)(2,1)} %get-tuple-element.22.grad, bf16[1024,1024]{1,0:T(8,128)(2,1)} %collective-permute-done.26.other), custom_call_target="tpu_custom_call" | custom-call | tf_op jit(solution)/shard_map/pallas_call | solution.py:168
  141.2 2.3 %collective-permute-start.27 = (bf16[256,1024]{1,0:T(8,128)(2,1)}, bf16[256,1024]{1,0:T(8,128)(2,1)S(1)}, u32[]{:S(2)}, u32[]{:S(2)}) collective-permute-start(bf16[256,1024]{1,0:T(8,128)(2,1)} %get-tuple-element.24), channel_id=1, source_target_pairs={{0,4},{2,6},{4,0},{6,2},{1,5},{3,7},{5,1},{7,3},{8,12},{10,14},{12... | collective-permute-start | bytes 1572872 | tf_op jit(solution)/shard_map/ppermute | solution.py:26
  143.5 2.0 %collective-permute-start.29 = (bf16[256,1024]{1,0:T(8,128)(2,1)}, bf16[256,1024]{1,0:T(8,128)(2,1)S(1)}, u32[]{:S(2)}, u32[]{:S(2)}) collective-permute-start(bf16[256,1024]{1,0:T(8,128)(2,1)} %get-tuple-element.26), channel_id=1, source_target_pairs={{0,6},{2,0},{4,2},{6,4},{1,7},{3,1},{5,3},{7,5},{8,14},{10,8},{12,... | collective-permute-start | bytes 1572872 | tf_op jit(solution)/shard_map/ppermute | solution.py:26
  146.5 11.2 %collective-permute-done.27 = bf16[256,1024]{1,0:T(8,128)(2,1)S(1)} collective-permute-done((bf16[256,1024]{1,0:T(8,128)(2,1)}, bf16[256,1024]{1,0:T(8,128)(2,1)S(1)}, u32[]{:S(2)}, u32[]{:S(2)}) %collective-permute-start.27) | collective-permute-done | bytes 524320 | tf_op jit(solution)/shard_map/ppermute | solution.py:26
  157.8 8.3 %collective-permute-done.28 = bf16[256,1024]{1,0:T(8,128)(2,1)S(1)} collective-permute-done((bf16[256,1024]{1,0:T(8,128)(2,1)}, bf16[256,1024]{1,0:T(8,128)(2,1)S(1)}, u32[]{:S(2)}, u32[]{:S(2)}) %collective-permute-start.28) | collective-permute-done | bytes 524320 | tf_op jit(solution)/shard_map/ppermute | solution.py:26
  166.1 2.5 %convert_add_fusion = f32[256,1024]{1,0:T(8,128)} fusion(bf16[256,1024]{1,0:T(8,128)(2,1)S(1)} %collective-permute-done.29, bf16[256,1024]{1,0:T(8,128)(2,1)S(1)} %collective-permute-done.28, f32[256,1024]{1,0:T(8,128)} %get-tuple-element.23, bf16[256,1024]{1,0:T(8,128)(2,1)S(1)} %collective-permute-done.27), kind=kLoop, calls=%fused_computation.10 | loop fusion | flops 1572864 | bytes 3670016 | tf_op jit(solution)/shard_map/add | solution.py:283
  (113 shorter events, 26.1 us)
Async XLA Ops:
  2.7 22.8 %collective-permute-start.7 = (bf16[24,2048]{1,0:T(8,128)(2,1)S(1)}, bf16[24,2048]{1,0:T(8,128)(2,1)S(1)}, u32[]{:S(2)}, u32[]{:S(2)}) collective-permute-start(bf16[24,2048]{1,0:T(8,128)(2,1)S(1)} %get-tuple-element.45), channel_id=1, source_target_pairs={{0,96},{32,128},{64,160},{96,192},{128,224},{160,0},{192,32},{224,... | collective-permute-start | bytes 294920 | tf_op jit(solution)/shard_map/ppermute | solution.py:26
  7.4 19.6 %collective-permute-start.6 = (bf16[24,2048]{1,0:T(8,128)(2,1)S(1)}, bf16[24,2048]{1,0:T(8,128)(2,1)}, u32[]{:S(2)}, u32[]{:S(2)}) collective-permute-start(bf16[24,2048]{1,0:T(8,128)(2,1)S(1)} %get-tuple-element.45), channel_id=1, source_target_pairs={{0,128},{32,160},{64,192},{96,224},{128,0},{160,32},{192,64},{224,... | collective-permute-start | bytes 294920 | tf_op jit(solution)/shard_map/ppermute | solution.py:26
  11.9 15.1 %collective-permute-start.5 = (bf16[24,2048]{1,0:T(8,128)(2,1)S(1)}, bf16[24,2048]{1,0:T(8,128)(2,1)}, u32[]{:S(2)}, u32[]{:S(2)}) collective-permute-start(bf16[24,2048]{1,0:T(8,128)(2,1)S(1)} %get-tuple-element.45), channel_id=1, source_target_pairs={{0,160},{32,192},{64,224},{96,0},{128,32},{160,64},{192,96},{224,1... | collective-permute-start | bytes 294920 | tf_op jit(solution)/shard_map/ppermute | solution.py:26
  15.0 14.6 %collective-permute-start.2 = (bf16[24,2048]{1,0:T(8,128)(2,1)S(1)}, bf16[24,2048]{1,0:T(8,128)(2,1)S(1)}, u32[]{:S(2)}, u32[]{:S(2)}) collective-permute-start(bf16[24,2048]{1,0:T(8,128)(2,1)S(1)} %get-tuple-element.45), channel_id=1, source_target_pairs={{0,8},{8,16},{16,24},{24,0},{1,9},{9,17},{17,25},{25,1},{2,10},{10... | collective-permute-start | bytes 294920 | tf_op jit(solution)/shard_map/ppermute | solution.py:26
  16.5 15.0 %collective-permute-start.1 = (bf16[24,2048]{1,0:T(8,128)(2,1)S(1)}, bf16[24,2048]{1,0:T(8,128)(2,1)S(1)}, u32[]{:S(2)}, u32[]{:S(2)}) collective-permute-start(bf16[24,2048]{1,0:T(8,128)(2,1)S(1)} %get-tuple-element.45), channel_id=1, source_target_pairs={{0,16},{8,24},{16,0},{24,8},{1,17},{9,25},{17,1},{25,9},{2,18},{10... | collective-permute-start | bytes 294920 | tf_op jit(solution)/shard_map/ppermute | solution.py:26
  25.5 5.9 %collective-permute-start = (bf16[24,2048]{1,0:T(8,128)(2,1)S(1)}, bf16[24,2048]{1,0:T(8,128)(2,1)S(1)}, u32[]{:S(2)}, u32[]{:S(2)}) collective-permute-start(bf16[24,2048]{1,0:T(8,128)(2,1)S(1)} %get-tuple-element.45), channel_id=1, source_target_pairs={{0,24},{8,0},{16,8},{24,16},{1,25},{9,1},{17,9},{25,17},{2,26},{10... | collective-permute-start | bytes 294920 | tf_op jit(solution)/shard_map/ppermute | solution.py:26
  28.0 18.8 %collective-permute-start.10 = (bf16[72,2048]{1,0:T(8,128)(2,1)S(1)}, bf16[72,2048]{1,0:T(8,128)(2,1)S(1)}, u32[]{:S(2)}, u32[]{:S(2)}) collective-permute-start(bf16[72,2048]{1,0:T(8,128)(2,1)S(1)} %pad_maximum_fusion.1), channel_id=1, source_target_pairs={{0,8},{8,16},{16,24},{24,0},{1,9},{9,17},{17,25},{25,1},{2,10},{10... | collective-permute-start | bytes 884744 | tf_op jit(solution)/shard_map/ppermute | solution.py:26
  28.6 18.1 %collective-permute-start.9 = (bf16[72,2048]{1,0:T(8,128)(2,1)S(1)}, bf16[72,2048]{1,0:T(8,128)(2,1)S(1)}, u32[]{:S(2)}, u32[]{:S(2)}) collective-permute-start(bf16[72,2048]{1,0:T(8,128)(2,1)S(1)} %pad_maximum_fusion.1), channel_id=1, source_target_pairs={{0,16},{8,24},{16,0},{24,8},{1,17},{9,25},{17,1},{25,9},{2,18},{10... | collective-permute-start | bytes 884744 | tf_op jit(solution)/shard_map/ppermute | solution.py:26
  29.6 17.1 %collective-permute-start.8 = (bf16[72,2048]{1,0:T(8,128)(2,1)S(1)}, bf16[72,2048]{1,0:T(8,128)(2,1)S(1)}, u32[]{:S(2)}, u32[]{:S(2)}) collective-permute-start(bf16[72,2048]{1,0:T(8,128)(2,1)S(1)} %pad_maximum_fusion.1), channel_id=1, source_target_pairs={{0,24},{8,0},{16,8},{24,16},{1,25},{9,1},{17,9},{25,17},{2,26},{10... | collective-permute-start | bytes 884744 | tf_op jit(solution)/shard_map/ppermute | solution.py:26
  31.5 11.8 %collective-permute-start.4 = (bf16[96,2048]{1,0:T(8,128)(2,1)S(1)}, bf16[96,2048]{1,0:T(8,128)(2,1)S(1)}, u32[]{:S(2)}, u32[]{:S(2)}) collective-permute-start(bf16[96,2048]{1,0:T(8,128)(2,1)S(1)} %pad_maximum_fusion), channel_id=1, source_target_pairs={{0,32},{32,64},{64,96},{96,128},{128,160},{160,192},{192,224},{224... | collective-permute-start | bytes 1179656 | tf_op jit(solution)/shard_map/ppermute | solution.py:26
  33.7 9.5 %collective-permute-start.3 = (bf16[96,2048]{1,0:T(8,128)(2,1)S(1)}, bf16[96,2048]{1,0:T(8,128)(2,1)S(1)}, u32[]{:S(2)}, u32[]{:S(2)}) collective-permute-start(bf16[96,2048]{1,0:T(8,128)(2,1)S(1)} %pad_maximum_fusion), channel_id=1, source_target_pairs={{0,224},{32,0},{64,32},{96,64},{128,96},{160,128},{192,160},{224,1... | collective-permute-start | bytes 1179656 | tf_op jit(solution)/shard_map/ppermute | solution.py:26
  43.4 10.0 %collective-permute-start.12 = (bf16[96,2048]{1,0:T(8,128)(2,1)S(1)}, bf16[96,2048]{1,0:T(8,128)(2,1)S(1)}, u32[]{:S(2)}, u32[]{:S(2)}) collective-permute-start(bf16[96,2048]{1,0:T(8,128)(2,1)S(1)} %collective-permute-done.4), channel_id=1, source_target_pairs={{0,32},{32,64},{64,96},{96,128},{128,160},{160,192},{192,224},{224... | collective-permute-start | bytes 1179656 | tf_op jit(solution)/shard_map/ppermute | solution.py:26
  43.8 8.8 %collective-permute-start.11 = (bf16[96,2048]{1,0:T(8,128)(2,1)S(1)}, bf16[96,2048]{1,0:T(8,128)(2,1)S(1)}, u32[]{:S(2)}, u32[]{:S(2)}) collective-permute-start(bf16[96,2048]{1,0:T(8,128)(2,1)S(1)} %collective-permute-done.3), channel_id=1, source_target_pairs={{0,224},{32,0},{64,32},{96,64},{128,96},{160,128},{192,160},{224,1... | collective-permute-start | bytes 1179656 | tf_op jit(solution)/shard_map/ppermute | solution.py:26
  61.3 15.1 %all-to-all-start = ((f32[32,1,896]{2,1,0:T(1,128)}), f32[32,1,896]{2,1,0:T(1,128)S(1)}, u32[]{:S(2)}, u32[]{:S(2)}) async-start(f32[32,1,896]{2,1,0:T(1,128)} %broadcast_in_dim.16), calls=%async_computation | async-start | bytes 229376 | tf_op jit(solution)/shard_map/all_to_all | solution.py:233
  87.4 14.2 %collective-permute-start.17 = (bf16[72,2048]{1,0:T(8,128)(2,1)}, bf16[72,2048]{1,0:T(8,128)(2,1)}, u32[]{:S(2)}, u32[]{:S(2)}) collective-permute-start(bf16[72,2048]{1,0:T(8,128)(2,1)} %get-tuple-element.19), channel_id=1, source_target_pairs={{0,8},{8,16},{16,24},{24,0},{1,9},{9,17},{17,25},{25,1},{2,10},{10... | collective-permute-start | bytes 884744 | tf_op jit(solution)/shard_map/ppermute | solution.py:26
  87.8 14.2 %collective-permute-start.18 = (bf16[72,2048]{1,0:T(8,128)(2,1)}, bf16[72,2048]{1,0:T(8,128)(2,1)}, u32[]{:S(2)}, u32[]{:S(2)}) collective-permute-start(bf16[72,2048]{1,0:T(8,128)(2,1)} %get-tuple-element.20), channel_id=1, source_target_pairs={{0,16},{8,24},{16,0},{24,8},{1,17},{9,25},{17,1},{25,9},{2,18},{10... | collective-permute-start | bytes 884744 | tf_op jit(solution)/shard_map/ppermute | solution.py:26
  90.4 11.6 %collective-permute-start.19 = (bf16[72,2048]{1,0:T(8,128)(2,1)}, bf16[72,2048]{1,0:T(8,128)(2,1)}, u32[]{:S(2)}, u32[]{:S(2)}) collective-permute-start(bf16[72,2048]{1,0:T(8,128)(2,1)} %get-tuple-element.21), channel_id=1, source_target_pairs={{0,24},{8,0},{16,8},{24,16},{1,25},{9,1},{17,9},{25,17},{2,26},{10... | collective-permute-start | bytes 884744 | tf_op jit(solution)/shard_map/ppermute | solution.py:26
  92.0 11.2 %collective-permute-start.13 = (bf16[96,2048]{1,0:T(8,128)(2,1)}, bf16[96,2048]{1,0:T(8,128)(2,1)S(1)}, u32[]{:S(2)}, u32[]{:S(2)}) collective-permute-start(bf16[96,2048]{1,0:T(8,128)(2,1)} %get-tuple-element.16), channel_id=1, source_target_pairs={{0,32},{32,64},{64,96},{96,128},{128,160},{160,192},{192,224},{224... | collective-permute-start | bytes 1179656 | tf_op jit(solution)/shard_map/ppermute | solution.py:26
  92.7 10.6 %collective-permute-start.15 = (bf16[96,2048]{1,0:T(8,128)(2,1)}, bf16[96,2048]{1,0:T(8,128)(2,1)}, u32[]{:S(2)}, u32[]{:S(2)}) collective-permute-start(bf16[96,2048]{1,0:T(8,128)(2,1)} %get-tuple-element.17), channel_id=1, source_target_pairs={{0,224},{32,0},{64,32},{96,64},{128,96},{160,128},{192,160},{224,1... | collective-permute-start | bytes 1179656 | tf_op jit(solution)/shard_map/ppermute | solution.py:26
  101.6 32.4 %collective-permute-start.26 = (bf16[1024,1024]{1,0:T(8,128)(2,1)}, bf16[1024,1024]{1,0:T(8,128)(2,1)}, u32[]{:S(2)}, u32[]{:S(2)}) collective-permute-start(bf16[1024,1024]{1,0:T(8,128)(2,1)} %shard_map.113), channel_id=1, source_target_pairs={{0,1},{1,0},{2,3},{3,2},{4,5},{5,4},{6,7},{7,6},{8,9},{9,8},{10,11... | collective-permute-start | bytes 6291464 | tf_op jit(solution)/shard_map/ppermute | solution.py:26
  103.3 30.5 %copy-start.4 = (bf16[24,1,2048]{2,0,1:T(8,128)(2,1)S(1)}, bf16[24,1,2048]{2,0,1:T(8,128)(2,1)}, u32[]{:S(2)}) copy-start(bf16[24,1,2048]{2,0,1:T(8,128)(2,1)} %param.9) | copy-start | bytes 294916
  104.6 19.4 %collective-permute-start.14 = (bf16[96,2048]{1,0:T(8,128)(2,1)S(1)}, bf16[96,2048]{1,0:T(8,128)(2,1)S(1)}, u32[]{:S(2)}, u32[]{:S(2)}) collective-permute-start(bf16[96,2048]{1,0:T(8,128)(2,1)S(1)} %get-tuple-element.46), channel_id=1, source_target_pairs={{0,32},{32,64},{64,96},{96,128},{128,160},{160,192},{192,224},{224... | collective-permute-start | bytes 1179656 | tf_op jit(solution)/shard_map/ppermute | solution.py:26
  104.7 19.3 %collective-permute-start.16 = (bf16[96,2048]{1,0:T(8,128)(2,1)S(1)}, bf16[96,2048]{1,0:T(8,128)(2,1)S(1)}, u32[]{:S(2)}, u32[]{:S(2)}) collective-permute-start(bf16[96,2048]{1,0:T(8,128)(2,1)S(1)} %get-tuple-element.47), channel_id=1, source_target_pairs={{0,224},{32,0},{64,32},{96,64},{128,96},{160,128},{192,160},{224,1... | collective-permute-start | bytes 1179656 | tf_op jit(solution)/shard_map/ppermute | solution.py:26
  107.9 18.6 %collective-permute-start.20 = (bf16[24,2048]{1,0:T(8,128)(2,1)S(1)}, bf16[24,2048]{1,0:T(8,128)(2,1)S(1)}, u32[]{:S(2)}, u32[]{:S(2)}) collective-permute-start(bf16[24,2048]{1,0:T(8,128)(2,1)S(1)} %get-tuple-element.51), channel_id=1, source_target_pairs={{0,128},{32,160},{64,192},{96,224},{128,0},{160,32},{192,64},{224,... | collective-permute-start | bytes 294920 | tf_op jit(solution)/shard_map/ppermute | solution.py:26
  109.1 18.8 %collective-permute-start.22 = (bf16[24,2048]{1,0:T(8,128)(2,1)S(1)}, bf16[24,2048]{1,0:T(8,128)(2,1)S(1)}, u32[]{:S(2)}, u32[]{:S(2)}) collective-permute-start(bf16[24,2048]{1,0:T(8,128)(2,1)S(1)} %get-tuple-element.52), channel_id=1, source_target_pairs={{0,160},{32,192},{64,224},{96,0},{128,32},{160,64},{192,96},{224,1... | collective-permute-start | bytes 294920 | tf_op jit(solution)/shard_map/ppermute | solution.py:26
  123.9 7.6 %collective-permute-start.21 = (bf16[24,2048]{1,0:T(8,128)(2,1)S(1)}, bf16[24,2048]{1,0:T(8,128)(2,1)S(1)}, u32[]{:S(2)}, u32[]{:S(2)}) collective-permute-start(bf16[24,2048]{1,0:T(8,128)(2,1)S(1)} %get-tuple-element.53), channel_id=1, source_target_pairs={{0,96},{32,128},{64,160},{96,192},{128,224},{160,0},{192,32},{224,... | collective-permute-start | bytes 294920 | tf_op jit(solution)/shard_map/ppermute | solution.py:26
  124.1 7.5 %collective-permute-start.23 = (bf16[24,2048]{1,0:T(8,128)(2,1)S(1)}, bf16[24,2048]{1,0:T(8,128)(2,1)S(1)}, u32[]{:S(2)}, u32[]{:S(2)}) collective-permute-start(bf16[24,2048]{1,0:T(8,128)(2,1)S(1)} %get-tuple-element.48), channel_id=1, source_target_pairs={{0,16},{8,24},{16,0},{24,8},{1,17},{9,25},{17,1},{25,9},{2,18},{10... | collective-permute-start | bytes 294920 | tf_op jit(solution)/shard_map/ppermute | solution.py:26
  126.5 5.1 %collective-permute-start.25 = (bf16[24,2048]{1,0:T(8,128)(2,1)S(1)}, bf16[24,2048]{1,0:T(8,128)(2,1)S(1)}, u32[]{:S(2)}, u32[]{:S(2)}) collective-permute-start(bf16[24,2048]{1,0:T(8,128)(2,1)S(1)} %get-tuple-element.49), channel_id=1, source_target_pairs={{0,24},{8,0},{16,8},{24,16},{1,25},{9,1},{17,9},{25,17},{2,26},{10... | collective-permute-start | bytes 294920 | tf_op jit(solution)/shard_map/ppermute | solution.py:26
  128.0 5.8 %collective-permute-start.24 = (bf16[24,2048]{1,0:T(8,128)(2,1)S(1)}, bf16[24,2048]{1,0:T(8,128)(2,1)S(1)}, u32[]{:S(2)}, u32[]{:S(2)}) collective-permute-start(bf16[24,2048]{1,0:T(8,128)(2,1)S(1)} %get-tuple-element.50), channel_id=1, source_target_pairs={{0,8},{8,16},{16,24},{24,0},{1,9},{9,17},{17,25},{25,1},{2,10},{10... | collective-permute-start | bytes 294920 | tf_op jit(solution)/shard_map/ppermute | solution.py:26
  141.2 16.5 %collective-permute-start.27 = (bf16[256,1024]{1,0:T(8,128)(2,1)}, bf16[256,1024]{1,0:T(8,128)(2,1)S(1)}, u32[]{:S(2)}, u32[]{:S(2)}) collective-permute-start(bf16[256,1024]{1,0:T(8,128)(2,1)} %get-tuple-element.24), channel_id=1, source_target_pairs={{0,4},{2,6},{4,0},{6,2},{1,5},{3,7},{5,1},{7,3},{8,12},{10,14},{12... | collective-permute-start | bytes 1572872 | tf_op jit(solution)/shard_map/ppermute | solution.py:26
  143.5 22.6 %collective-permute-start.28 = (bf16[256,1024]{1,0:T(8,128)(2,1)}, bf16[256,1024]{1,0:T(8,128)(2,1)S(1)}, u32[]{:S(2)}, u32[]{:S(2)}) collective-permute-start(bf16[256,1024]{1,0:T(8,128)(2,1)} %get-tuple-element.25), channel_id=1, source_target_pairs={{0,2},{2,4},{4,6},{6,0},{1,3},{3,5},{5,7},{7,1},{8,10},{10,12},{12... | collective-permute-start | bytes 1572872 | tf_op jit(solution)/shard_map/ppermute | solution.py:26
  143.5 22.6 %collective-permute-start.29 = (bf16[256,1024]{1,0:T(8,128)(2,1)}, bf16[256,1024]{1,0:T(8,128)(2,1)S(1)}, u32[]{:S(2)}, u32[]{:S(2)}) collective-permute-start(bf16[256,1024]{1,0:T(8,128)(2,1)} %get-tuple-element.26), channel_id=1, source_target_pairs={{0,6},{2,0},{4,2},{6,4},{1,7},{3,1},{5,3},{7,5},{8,14},{10,8},{12,... | collective-permute-start | bytes 1572872 | tf_op jit(solution)/shard_map/ppermute | solution.py:26
  (11 other events, 170.7 us)

commit v2 on v0

--- a/solution.py
+++ b/solution.py
@@ -55,21 +55,25 @@
     left = vectors - high.astype(f32)
     middle = left.astype(bf16)
     low = (left - middle.astype(f32)).astype(bf16)
-    return sum(
-        lax.dot_general(order, part, (((1,), (1,)), ((), ())), preferred_element_type=f32)
-        for part in (high, middle, low)
-    )
+    count = vectors.shape[0]
+    parts = jnp.concatenate([high.astype(f32), middle.astype(f32), low.astype(f32)])
+    moved_parts = lax.dot_general(
+        order, parts.astype(bf16), (((1,), (1,)), ((), ())), preferred_element_type=f32
+    )
+    return [
+        sum(moved_parts[:, k + count * part : k + count * part + 1] for part in range(3))
+        for k in range(3)
+    ]
 
 
 def gradient_kernel(
     scores, matrix, order, vectors, grad, far_own, near, upward, downward, *far_away
 ):
-    columns = column_vectors(order[...], vectors[...])
-    log_total, weights, target = columns[:, 0:1], columns[:, 1:2], columns[:, 2:3]
+    log_total, weights, target = column_vectors(order[...], vectors[...])
     scale = weights * (1.0 + 2.0 * penalty * log_total)
     target = target.astype(jnp.int32)
     rows, width = scores.shape
-    step = 256
+    step = 128
     for low in range(0, width, step):
         part = slice(low, low + step)
         ids = lax.broadcasted_iota(jnp.int32, (rows, step), 1) + low
@@ -79,6 +83,7 @@
         ).astype(bf16)
 
     block, wide = upward.shape[0], far_own.shape[0]
+    step = 512
 
     def body(number, carry):
         part = pl.ds(pl.multiple_of(number * step, step), step)
@@ -126,6 +131,9 @@
         ref[...] = product.astype(ref.dtype)
 
 
+SMALL = pltpu.CompilerParams(vmem_limit_bytes=8 * 2**20)
+
+
 def shaped(*shapes):
     return tuple(jax.ShapeDtypeStruct(dims, kind) for dims, kind in shapes)
 
@@ -154,8 +162,9 @@
     threes = {kx: taken_from(three, "vp_1", kx) for kx in (2, 1, 3)}
     up2 = taken_from(up1, "vp_0", 1)
     down2 = taken_from(down1, "vp_0", -1)
+    early = [line, up1, down1, three] + [threes[kx] for kx in range(1, NX)]
     rows_all = jnp.concatenate(
-        [line, up1, down1, three] + [threes[kx] for kx in range(1, NX)] + [up2, down2]
+        lax.optimization_barrier(early) + [up2, down2]
     )
 
     place_z, place_x = lax.axis_index("vp_0"), lax.axis_index("vp_1")
@@ -212,6 +221,7 @@
         ),
         in_specs=spaces(0, 4),
         out_specs=spaces(0, 5 + NX - 1),
+        compiler_params=SMALL,
     )(scores, vocab_matrix, order, vectors)
     from_below = sent_to(upward, "vp_0", 1)
     from_above = sent_to(downward, "vp_0", -1)
@@ -224,6 +234,7 @@
         out_shape=shaped(((NY * share, columns), bf16)),
         in_specs=spaces(1, 2),
         out_specs=spaces(0, 1),
+        compiler_params=SMALL,
     )(place, rows_all, score_grad)
     other = taken_from(other, "dp_1", 1)
     vocab_grad, *away = pl.pallas_call(
@@ -233,6 +244,7 @@
         ),
         in_specs=spaces(1, 3),
         out_specs=spaces(0, NY),
+        compiler_params=SMALL,
     )(place, rows_all, score_grad, other)
     chip_y = {k: sent_to(away[k - 1], "dp_0", k) for k in (2, 1, 3)}
     above, below = near[block : 2 * block], near[2 * block :]

time: 171 us -> 172 us (level)
  the two profiles are of different devices: /device:TPU:8 before, /device:TPU:32 now
where the time goes in v2:
time: 172 us; the launch traced here: 171 us
  waiting for transfers between devices  66.6 us (39%)
  starting transfers between devices  60.8 us (35%)
  local copies, waits for them, and re-layouts  15.3 us (9%)
  Pallas kernels  12.1 us (7%)
  other arithmetic  10.8 us (6%)
  matrix products  4.71 us (3%)
    ppermute x30, waiting for transfers between devices, taken_from(): lax.ppermute(array, axis, [(i, (i - step) % count) for i in range(count)])  57.2 us
    ppermute x30, starting transfers between devices, taken_from(): lax.ppermute(array, axis, [(i, (i - step) % count) for i in range(count)])  51.4 us
    unnamed x48, local copies, waits for them, and re-layouts  14.2 us
    all_to_all x1, starting transfers between devices, whole(): lax.all_to_all(packed, VP, split_axis=0, concat_axis=0, tiled=True)[:, 0]  9.43 us
    all_to_all x1, waiting for transfers between devices, whole(): lax.all_to_all(packed, VP, split_axis=0, concat_axis=0, tiled=True)[:, 0]  9.39 us
    pallas_call x1, Pallas kernels, whole(): pl.pallas_call(gradient_kernel, out_shape=shaped(((total_rows, columns),...  6.66 us
    dot_general x1, matrix products, whole(): jnp.dot(rows_all, vocab_matrix, preferred_element_type=f32)  3.56 us
  transfers between devices with their start and end apart: 31, of which 16 were waited for; matrix products, arithmetic and copies ran while one was open for 5% of the time, Pallas kernels for 2%

profile of v2, /device:TPU:32, one launch (start us, length us, event | category | flops | bytes accessed | tf_op | source)
XLA Modules:
  0.0 171.3 jit_solution(4498313752037918626)
XLA Ops:
  2.7 5.9 %collective-permute-start.7 = (bf16[24,2048]{1,0:T(8,128)(2,1)S(1)}, bf16[24,2048]{1,0:T(8,128)(2,1)S(1)}, u32[]{:S(2)}, u32[]{:S(2)}) collective-permute-start(bf16[24,2048]{1,0:T(8,128)(2,1)S(1)} %fusion.8), channel_id=1, source_target_pairs={{0,96},{32,128},{64,160},{96,192},{128,224},{160,0},{192,32},{224,... | collective-permute-start | bytes 294920 | tf_op jit(solution)/shard_map/ppermute | solution.py:26
  9.1 1.5 collective-permute-start.2
  10.6 2.7 %collective-permute-start.1 = (bf16[24,2048]{1,0:T(8,128)(2,1)S(1)}, bf16[24,2048]{1,0:T(8,128)(2,1)S(1)}, u32[]{:S(2)}, u32[]{:S(2)}) collective-permute-start(bf16[24,2048]{1,0:T(8,128)(2,1)S(1)} %fusion.8), channel_id=1, source_target_pairs={{0,16},{8,24},{16,0},{24,8},{1,17},{9,25},{17,1},{25,9},{2,18},{10... | collective-permute-start | bytes 294920 | tf_op jit(solution)/shard_map/ppermute | solution.py:26
  13.3 1.4 collective-permute-start
  16.9 5.0 %collective-permute-start.5 = (bf16[24,2048]{1,0:T(8,128)(2,1)S(1)}, bf16[24,2048]{1,0:T(8,128)(2,1)S(1)}, u32[]{:S(2)}, u32[]{:S(2)}) collective-permute-start(bf16[24,2048]{1,0:T(8,128)(2,1)S(1)} %fusion.8), channel_id=1, source_target_pairs={{0,160},{32,192},{64,224},{96,0},{128,32},{160,64},{192,96},{224,1... | collective-permute-start | bytes 294920 | tf_op jit(solution)/shard_map/ppermute | solution.py:26
  24.0 4.5 %collective-permute-done.5 = bf16[24,2048]{1,0:T(8,128)(2,1)S(1)} collective-permute-done((bf16[24,2048]{1,0:T(8,128)(2,1)S(1)}, bf16[24,2048]{1,0:T(8,128)(2,1)S(1)}, u32[]{:S(2)}, u32[]{:S(2)}) %collective-permute-start.5) | collective-permute-done | bytes 98336 | tf_op jit(solution)/shard_map/ppermute | solution.py:26
  29.7 2.4 %collective-permute-start.8 = (bf16[72,2048]{1,0:T(8,128)(2,1)S(1)}, bf16[72,2048]{1,0:T(8,128)(2,1)S(1)}, u32[]{:S(2)}, u32[]{:S(2)}) collective-permute-start(bf16[72,2048]{1,0:T(8,128)(2,1)S(1)} %pad_maximum_fusion.1), channel_id=1, source_target_pairs={{0,24},{8,0},{16,8},{24,16},{1,25},{9,1},{17,9},{25,17},{2,26},{10... | collective-permute-start | bytes 884744 | tf_op jit(solution)/shard_map/ppermute | solution.py:26
  33.4 6.8 %collective-permute-done.10 = bf16[72,2048]{1,0:T(8,128)(2,1)S(1)} collective-permute-done((bf16[72,2048]{1,0:T(8,128)(2,1)S(1)}, bf16[72,2048]{1,0:T(8,128)(2,1)S(1)}, u32[]{:S(2)}, u32[]{:S(2)}) %collective-permute-start.10) | collective-permute-done | bytes 294944 | tf_op jit(solution)/shard_map/ppermute | solution.py:26
  40.8 4.5 %collective-permute-start.12 = (bf16[96,2048]{1,0:T(8,128)(2,1)S(1)}, bf16[96,2048]{1,0:T(8,128)(2,1)S(1)}, u32[]{:S(2)}, u32[]{:S(2)}) collective-permute-start(bf16[96,2048]{1,0:T(8,128)(2,1)S(1)} %collective-permute-done.4), channel_id=1, source_target_pairs={{0,32},{32,64},{64,96},{96,128},{128,160},{160,192},{192,224},{224... | collective-permute-start | bytes 1179656 | tf_op jit(solution)/shard_map/ppermute | solution.py:26
  45.4 9.1 %collective-permute-done.11 = bf16[96,2048]{1,0:T(8,128)(2,1)S(1)} collective-permute-done((bf16[96,2048]{1,0:T(8,128)(2,1)S(1)}, bf16[96,2048]{1,0:T(8,128)(2,1)S(1)}, u32[]{:S(2)}, u32[]{:S(2)}) %collective-permute-start.11) | collective-permute-done | bytes 393248 | tf_op jit(solution)/shard_map/ppermute | solution.py:26
  54.5 3.6 %fusion.41 = (f32[768]{0:T(1024)S(1)}, f32[768,1024]{1,0:T(8,128)S(1)}) fusion(f32[1024]{0:T(1024)S(1)} %copy-done.18, bf16[768,2048]{1,0:T(8,128)(2,1)S(1)} %constant_dynamic-update-slice_fusion.rows, bf16[2048,1024]{1,0:T(8,128)(2,1)S(1)} %copy-done.6), kind=kOutput, calls=%fused_computation.110 | convolution fusion | flops 3222797568 | bytes 10492928 | tf_op jit(solution)/shard_map/dot_general | solution.py:184
  59.2 1.6 copy-done
  62.4 9.4 %all-to-all-start = ((f32[32,1,896]{2,1,0:T(1,128)}), f32[32,1,896]{2,1,0:T(1,128)S(1)}, u32[]{:S(2)}, u32[]{:S(2)}) async-start(f32[32,1,896]{2,1,0:T(1,128)} %broadcast_in_dim.16), calls=%async_computation | async-start | bytes 229376 | tf_op jit(solution)/shard_map/all_to_all | solution.py:194
  71.9 9.4 %all-to-all-done = f32[32,1,896]{2,1,0:T(1,128)S(1)} async-done(((f32[32,1,896]{2,1,0:T(1,128)}), f32[32,1,896]{2,1,0:T(1,128)S(1)}, u32[]{:S(2)}, u32[]{:S(2)}) %all-to-all-start) | async-done | bytes 114720 | tf_op jit(solution)/shard_map/all_to_all | solution.py:194
  82.0 1.9 %copy-done.1 = f32[768,1024]{1,0:T(8,128)S(1)} copy-done((f32[768,1024]{1,0:T(8,128)S(1)}, f32[768,1024]{1,0:T(8,128)}, u32[]{:S(2)}) %copy-start.1) | copy-done | bytes 3145752
  85.2 2.2 %copy-done.7 = bf16[2048,1024]{1,0:T(8,128)(2,1)S(1)} copy-done((bf16[2048,1024]{1,0:T(8,128)(2,1)S(1)}, bf16[2048,1024]{1,0:T(8,128)(2,1)}, u32[]{:S(2)}) %copy-start.7) | copy-done | bytes 4194328
  87.3 6.7 %shard_map.112 = (bf16[768,1024]{1,0:T(8,128)(2,1)S(1)}, f32[72,2048]{1,0:T(8,128)S(1)}, f32[288,2048]{1,0:T(8,128)S(1)}, bf16[96,2048]{1,0:T(8,128)(2,1)S(1)}, ...) custom-call(f32[768,1024]{1,0:T(8,128)S(1)} %copy-done.1, ...), custom_call_target="tpu_custom_call" | custom-call | tf_op jit(solution)/shard_map/pallas_call | solution.py:212
  98.8 2.2 %collective-permute-start.18 = (bf16[72,2048]{1,0:T(8,128)(2,1)}, bf16[72,2048]{1,0:T(8,128)(2,1)}, u32[]{:S(2)}, u32[]{:S(2)}) collective-permute-start(bf16[72,2048]{1,0:T(8,128)(2,1)} %get-tuple-element.34), channel_id=1, source_target_pairs={{0,16},{8,24},{16,0},{24,8},{1,17},{9,25},{17,1},{25,9},{2,18},{10... | collective-permute-start | bytes 884744 | tf_op jit(solution)/shard_map/ppermute | solution.py:26
  105.3 3.1 %shard_map.113 = bf16[1024,1024]{1,0:T(8,128)(2,1)S(1)} custom-call(s32[2]{0:T(128)S(1)} %pad_add_fusion.place, bf16[768,2048]{1,0:T(8,128)(2,1)S(1)} %constant_dynamic-update-slice_fusion.rows, bf16[768,1024]{1,0:T(8,128)(2,1)S(1)} %copy-done.3), custom_call_target="tpu_custom_call" | custom-call | tf_op jit(solution)/shard_map/pallas_call | solution.py:232
  109.1 3.5 %collective-permute-done.17 = bf16[72,2048]{1,0:T(8,128)(2,1)} collective-permute-done((bf16[72,2048]{1,0:T(8,128)(2,1)}, bf16[72,2048]{1,0:T(8,128)(2,1)}, u32[]{:S(2)}, u32[]{:S(2)}) %collective-permute-start.17) | collective-permute-done | bytes 294944 | tf_op jit(solution)/shard_map/ppermute | solution.py:26
  116.9 1.7 %collective-permute-start.20 = (bf16[24,2048]{1,0:T(8,128)(2,1)S(1)}, bf16[24,2048]{1,0:T(8,128)(2,1)S(1)}, u32[]{:S(2)}, u32[]{:S(2)}) collective-permute-start(bf16[24,2048]{1,0:T(8,128)(2,1)S(1)} %get-tuple-element.63), channel_id=1, source_target_pairs={{0,128},{32,160},{64,192},{96,224},{128,0},{160,32},{192,64},{224,... | collective-permute-start | bytes 294920 | tf_op jit(solution)/shard_map/ppermute | solution.py:26
  118.6 3.7 %collective-permute-start.22 = (bf16[24,2048]{1,0:T(8,128)(2,1)S(1)}, bf16[24,2048]{1,0:T(8,128)(2,1)S(1)}, u32[]{:S(2)}, u32[]{:S(2)}) collective-permute-start(bf16[24,2048]{1,0:T(8,128)(2,1)S(1)} %get-tuple-element.64), channel_id=1, source_target_pairs={{0,160},{32,192},{64,224},{96,0},{128,32},{160,64},{192,96},{224,1... | collective-permute-start | bytes 294920 | tf_op jit(solution)/shard_map/ppermute | solution.py:26
  122.2 4.9 %collective-permute-done.14 = bf16[96,2048]{1,0:T(8,128)(2,1)S(1)} collective-permute-done((bf16[96,2048]{1,0:T(8,128)(2,1)S(1)}, bf16[96,2048]{1,0:T(8,128)(2,1)S(1)}, u32[]{:S(2)}, u32[]{:S(2)}) %collective-permute-start.14) | collective-permute-done | bytes 393248 | tf_op jit(solution)/shard_map/ppermute | solution.py:26
  128.5 5.2 %collective-permute-done.16 = bf16[96,2048]{1,0:T(8,128)(2,1)S(1)} collective-permute-done((bf16[96,2048]{1,0:T(8,128)(2,1)S(1)}, bf16[96,2048]{1,0:T(8,128)(2,1)S(1)}, u32[]{:S(2)}, u32[]{:S(2)}) %collective-permute-start.16) | collective-permute-done | bytes 393248 | tf_op jit(solution)/shard_map/ppermute | solution.py:26
  134.7 1.9 %collective-permute-done.20 = bf16[24,2048]{1,0:T(8,128)(2,1)S(1)} collective-permute-done((bf16[24,2048]{1,0:T(8,128)(2,1)S(1)}, bf16[24,2048]{1,0:T(8,128)(2,1)S(1)}, u32[]{:S(2)}, u32[]{:S(2)}) %collective-permute-start.20) | collective-permute-done | bytes 98336 | tf_op jit(solution)/shard_map/ppermute | solution.py:26
  136.6 2.3 %collective-permute-start.25 = (bf16[24,2048]{1,0:T(8,128)(2,1)S(1)}, bf16[24,2048]{1,0:T(8,128)(2,1)S(1)}, u32[]{:S(2)}, u32[]{:S(2)}) collective-permute-start(bf16[24,2048]{1,0:T(8,128)(2,1)S(1)} %get-tuple-element.61), channel_id=1, source_target_pairs={{0,24},{8,0},{16,8},{24,16},{1,25},{9,1},{17,9},{25,17},{2,26},{10... | collective-permute-start | bytes 294920 | tf_op jit(solution)/shard_map/ppermute | solution.py:26
  141.2 3.5 %collective-permute-done.24 = bf16[24,2048]{1,0:T(8,128)(2,1)S(1)} collective-permute-done((bf16[24,2048]{1,0:T(8,128)(2,1)S(1)}, bf16[24,2048]{1,0:T(8,128)(2,1)S(1)}, u32[]{:S(2)}, u32[]{:S(2)}) %collective-permute-start.24) | collective-permute-done | bytes 98336 | tf_op jit(solution)/shard_map/ppermute | solution.py:26
  144.9 2.4 %shard_map.114 = (f32[256,1024]{1,0:T(8,128)S(1)}, bf16[256,1024]{1,0:T(8,128)(2,1)S(1)}, bf16[256,1024]{1,0:T(8,128)(2,1)S(1)}, bf16[256,1024]{1,0:T(8,128)(2,1)S(1)}) custom-call(s32[2]{0:T(128)S(1)} %pad_add_fusion.place, bf16[768,2048]{1,0:T(8,128)(2,1)S(1)} %constant_dynamic-update-slice_fusion.rows, bf16[768,1024]{1,0:T(8,128)(2,1)S(1)} %copy-done.4, ...), custom_call_target="tpu_custom_call" | custom-call | tf_op jit(solution)/shard_map/pallas_call | solution.py:240
  147.3 3.3 %collective-permute-start.27 = (bf16[256,1024]{1,0:T(8,128)(2,1)S(1)}, bf16[256,1024]{1,0:T(8,128)(2,1)S(1)}, u32[]{:S(2)}, u32[]{:S(2)}) collective-permute-start(bf16[256,1024]{1,0:T(8,128)(2,1)S(1)} %get-tuple-element.38), channel_id=1, source_target_pairs={{0,4},{2,6},{4,0},{6,2},{1,5},{3,7},{5,1},{7,3},{8,12},{10,14},{12... | collective-permute-start | bytes 1572872 | tf_op jit(solution)/shard_map/ppermute | solution.py:26
  151.3 2.6 %collective-permute-start.29 = (bf16[256,1024]{1,0:T(8,128)(2,1)S(1)}, bf16[256,1024]{1,0:T(8,128)(2,1)S(1)}, u32[]{:S(2)}, u32[]{:S(2)}) collective-permute-start(bf16[256,1024]{1,0:T(8,128)(2,1)S(1)} %get-tuple-element.40), channel_id=1, source_target_pairs={{0,6},{2,0},{4,2},{6,4},{1,7},{3,1},{5,3},{7,5},{8,14},{10,8},{12,... | collective-permute-start | bytes 1572872 | tf_op jit(solution)/shard_map/ppermute | solution.py:26
  154.9 8.9 %collective-permute-done.27 = bf16[256,1024]{1,0:T(8,128)(2,1)S(1)} collective-permute-done((bf16[256,1024]{1,0:T(8,128)(2,1)S(1)}, bf16[256,1024]{1,0:T(8,128)(2,1)S(1)}, u32[]{:S(2)}, u32[]{:S(2)}) %collective-permute-start.27) | collective-permute-done | bytes 524320 | tf_op jit(solution)/shard_map/ppermute | solution.py:26
  163.7 5.8 %collective-permute-done.28 = bf16[256,1024]{1,0:T(8,128)(2,1)S(1)} collective-permute-done((bf16[256,1024]{1,0:T(8,128)(2,1)S(1)}, bf16[256,1024]{1,0:T(8,128)(2,1)S(1)}, u32[]{:S(2)}, u32[]{:S(2)}) %collective-permute-start.28) | collective-permute-done | bytes 524320 | tf_op jit(solution)/shard_map/ppermute | solution.py:26
  (125 shorter events, 36.8 us)
Async XLA Ops:
  2.7 21.3 %collective-permute-start.7 = (bf16[24,2048]{1,0:T(8,128)(2,1)S(1)}, bf16[24,2048]{1,0:T(8,128)(2,1)S(1)}, u32[]{:S(2)}, u32[]{:S(2)}) collective-permute-start(bf16[24,2048]{1,0:T(8,128)(2,1)S(1)} %fusion.8), channel_id=1, source_target_pairs={{0,96},{32,128},{64,160},{96,192},{128,224},{160,0},{192,32},{224,... | collective-permute-start | bytes 294920 | tf_op jit(solution)/shard_map/ppermute | solution.py:26
  8.6 15.4 %collective-permute-start.6 = (bf16[24,2048]{1,0:T(8,128)(2,1)S(1)}, bf16[24,2048]{1,0:T(8,128)(2,1)S(1)}, u32[]{:S(2)}, u32[]{:S(2)}) collective-permute-start(bf16[24,2048]{1,0:T(8,128)(2,1)S(1)} %fusion.8), channel_id=1, source_target_pairs={{0,128},{32,160},{64,192},{96,224},{128,0},{160,32},{192,64},{224,... | collective-permute-start | bytes 294920 | tf_op jit(solution)/shard_map/ppermute | solution.py:26
  9.1 7.7 %collective-permute-start.2 = (bf16[24,2048]{1,0:T(8,128)(2,1)S(1)}, bf16[24,2048]{1,0:T(8,128)(2,1)S(1)}, u32[]{:S(2)}, u32[]{:S(2)}) collective-permute-start(bf16[24,2048]{1,0:T(8,128)(2,1)S(1)} %fusion.8), channel_id=1, source_target_pairs={{0,8},{8,16},{16,24},{24,0},{1,9},{9,17},{17,25},{25,1},{2,10},{10... | collective-permute-start | bytes 294920 | tf_op jit(solution)/shard_map/ppermute | solution.py:26
  10.6 11.2 %collective-permute-start.1 = (bf16[24,2048]{1,0:T(8,128)(2,1)S(1)}, bf16[24,2048]{1,0:T(8,128)(2,1)S(1)}, u32[]{:S(2)}, u32[]{:S(2)}) collective-permute-start(bf16[24,2048]{1,0:T(8,128)(2,1)S(1)} %fusion.8), channel_id=1, source_target_pairs={{0,16},{8,24},{16,0},{24,8},{1,17},{9,25},{17,1},{25,9},{2,18},{10... | collective-permute-start | bytes 294920 | tf_op jit(solution)/shard_map/ppermute | solution.py:26
  13.3 8.5 %collective-permute-start = (bf16[24,2048]{1,0:T(8,128)(2,1)S(1)}, bf16[24,2048]{1,0:T(8,128)(2,1)S(1)}, u32[]{:S(2)}, u32[]{:S(2)}) collective-permute-start(bf16[24,2048]{1,0:T(8,128)(2,1)S(1)} %fusion.8), channel_id=1, source_target_pairs={{0,24},{8,0},{16,8},{24,16},{1,25},{9,1},{17,9},{25,17},{2,26},{10... | collective-permute-start | bytes 294920 | tf_op jit(solution)/shard_map/ppermute | solution.py:26
  16.9 11.6 %collective-permute-start.5 = (bf16[24,2048]{1,0:T(8,128)(2,1)S(1)}, bf16[24,2048]{1,0:T(8,128)(2,1)S(1)}, u32[]{:S(2)}, u32[]{:S(2)}) collective-permute-start(bf16[24,2048]{1,0:T(8,128)(2,1)S(1)} %fusion.8), channel_id=1, source_target_pairs={{0,160},{32,192},{64,224},{96,0},{128,32},{160,64},{192,96},{224,1... | collective-permute-start | bytes 294920 | tf_op jit(solution)/shard_map/ppermute | solution.py:26
  21.9 18.7 %collective-permute-start.4 = (bf16[96,2048]{1,0:T(8,128)(2,1)S(1)}, bf16[96,2048]{1,0:T(8,128)(2,1)S(1)}, u32[]{:S(2)}, u32[]{:S(2)}) collective-permute-start(bf16[96,2048]{1,0:T(8,128)(2,1)S(1)} %pad_maximum_fusion), channel_id=1, source_target_pairs={{0,32},{32,64},{64,96},{96,128},{128,160},{160,192},{192,224},{224... | collective-permute-start | bytes 1179656 | tf_op jit(solution)/shard_map/ppermute | solution.py:26
  23.0 17.7 %collective-permute-start.3 = (bf16[96,2048]{1,0:T(8,128)(2,1)S(1)}, bf16[96,2048]{1,0:T(8,128)(2,1)S(1)}, u32[]{:S(2)}, u32[]{:S(2)}) collective-permute-start(bf16[96,2048]{1,0:T(8,128)(2,1)S(1)} %pad_maximum_fusion), channel_id=1, source_target_pairs={{0,224},{32,0},{64,32},{96,64},{128,96},{160,128},{192,160},{224,1... | collective-permute-start | bytes 1179656 | tf_op jit(solution)/shard_map/ppermute | solution.py:26
  28.5 11.7 %collective-permute-start.10 = (bf16[72,2048]{1,0:T(8,128)(2,1)S(1)}, bf16[72,2048]{1,0:T(8,128)(2,1)S(1)}, u32[]{:S(2)}, u32[]{:S(2)}) collective-permute-start(bf16[72,2048]{1,0:T(8,128)(2,1)S(1)} %pad_maximum_fusion.1), channel_id=1, source_target_pairs={{0,8},{8,16},{16,24},{24,0},{1,9},{9,17},{17,25},{25,1},{2,10},{10... | collective-permute-start | bytes 884744 | tf_op jit(solution)/shard_map/ppermute | solution.py:26
  29.2 11.1 %collective-permute-start.9 = (bf16[72,2048]{1,0:T(8,128)(2,1)S(1)}, bf16[72,2048]{1,0:T(8,128)(2,1)S(1)}, u32[]{:S(2)}, u32[]{:S(2)}) collective-permute-start(bf16[72,2048]{1,0:T(8,128)(2,1)S(1)} %pad_maximum_fusion.1), channel_id=1, source_target_pairs={{0,16},{8,24},{16,0},{24,8},{1,17},{9,25},{17,1},{25,9},{2,18},{10... | collective-permute-start | bytes 884744 | tf_op jit(solution)/shard_map/ppermute | solution.py:26
  29.7 10.9 %collective-permute-start.8 = (bf16[72,2048]{1,0:T(8,128)(2,1)S(1)}, bf16[72,2048]{1,0:T(8,128)(2,1)S(1)}, u32[]{:S(2)}, u32[]{:S(2)}) collective-permute-start(bf16[72,2048]{1,0:T(8,128)(2,1)S(1)} %pad_maximum_fusion.1), channel_id=1, source_target_pairs={{0,24},{8,0},{16,8},{24,16},{1,25},{9,1},{17,9},{25,17},{2,26},{10... | collective-permute-start | bytes 884744 | tf_op jit(solution)/shard_map/ppermute | solution.py:26
  40.8 13.7 %collective-permute-start.12 = (bf16[96,2048]{1,0:T(8,128)(2,1)S(1)}, bf16[96,2048]{1,0:T(8,128)(2,1)S(1)}, u32[]{:S(2)}, u32[]{:S(2)}) collective-permute-start(bf16[96,2048]{1,0:T(8,128)(2,1)S(1)} %collective-permute-done.4), channel_id=1, source_target_pairs={{0,32},{32,64},{64,96},{96,128},{128,160},{160,192},{192,224},{224... | collective-permute-start | bytes 1179656 | tf_op jit(solution)/shard_map/ppermute | solution.py:26
  45.3 9.1 %collective-permute-start.11 = (bf16[96,2048]{1,0:T(8,128)(2,1)S(1)}, bf16[96,2048]{1,0:T(8,128)(2,1)S(1)}, u32[]{:S(2)}, u32[]{:S(2)}) collective-permute-start(bf16[96,2048]{1,0:T(8,128)(2,1)S(1)} %collective-permute-done.3), channel_id=1, source_target_pairs={{0,224},{32,0},{64,32},{96,64},{128,96},{160,128},{192,160},{224,1... | collective-permute-start | bytes 1179656 | tf_op jit(solution)/shard_map/ppermute | solution.py:26
  62.4 18.9 %all-to-all-start = ((f32[32,1,896]{2,1,0:T(1,128)}), f32[32,1,896]{2,1,0:T(1,128)S(1)}, u32[]{:S(2)}, u32[]{:S(2)}) async-start(f32[32,1,896]{2,1,0:T(1,128)} %broadcast_in_dim.16), calls=%async_computation | async-start | bytes 229376 | tf_op jit(solution)/shard_map/all_to_all | solution.py:194
  98.2 14.4 %collective-permute-start.17 = (bf16[72,2048]{1,0:T(8,128)(2,1)}, bf16[72,2048]{1,0:T(8,128)(2,1)}, u32[]{:S(2)}, u32[]{:S(2)}) collective-permute-start(bf16[72,2048]{1,0:T(8,128)(2,1)} %get-tuple-element.33), channel_id=1, source_target_pairs={{0,8},{8,16},{16,24},{24,0},{1,9},{9,17},{17,25},{25,1},{2,10},{10... | collective-permute-start | bytes 884744 | tf_op jit(solution)/shard_map/ppermute | solution.py:26
  98.8 13.8 %collective-permute-start.18 = (bf16[72,2048]{1,0:T(8,128)(2,1)}, bf16[72,2048]{1,0:T(8,128)(2,1)}, u32[]{:S(2)}, u32[]{:S(2)}) collective-permute-start(bf16[72,2048]{1,0:T(8,128)(2,1)} %get-tuple-element.34), channel_id=1, source_target_pairs={{0,16},{8,24},{16,0},{24,8},{1,17},{9,25},{17,1},{25,9},{2,18},{10... | collective-permute-start | bytes 884744 | tf_op jit(solution)/shard_map/ppermute | solution.py:26
  101.0 12.2 %collective-permute-start.19 = (bf16[72,2048]{1,0:T(8,128)(2,1)}, bf16[72,2048]{1,0:T(8,128)(2,1)}, u32[]{:S(2)}, u32[]{:S(2)}) collective-permute-start(bf16[72,2048]{1,0:T(8,128)(2,1)} %get-tuple-element.35), channel_id=1, source_target_pairs={{0,24},{8,0},{16,8},{24,16},{1,25},{9,1},{17,9},{25,17},{2,26},{10... | collective-permute-start | bytes 884744 | tf_op jit(solution)/shard_map/ppermute | solution.py:26
  101.8 12.6 %collective-permute-start.13 = (bf16[96,2048]{1,0:T(8,128)(2,1)}, bf16[96,2048]{1,0:T(8,128)(2,1)S(1)}, u32[]{:S(2)}, u32[]{:S(2)}) collective-permute-start(bf16[96,2048]{1,0:T(8,128)(2,1)} %copy-done.12), channel_id=1, source_target_pairs={{0,32},{32,64},{64,96},{96,128},{128,160},{160,192},{192,224},{224... | collective-permute-start | bytes 1179656 | tf_op jit(solution)/shard_map/ppermute | solution.py:26
  102.5 12.0 %collective-permute-start.15 = (bf16[96,2048]{1,0:T(8,128)(2,1)S(1)}, bf16[96,2048]{1,0:T(8,128)(2,1)S(1)}, u32[]{:S(2)}, u32[]{:S(2)}) collective-permute-start(bf16[96,2048]{1,0:T(8,128)(2,1)S(1)} %get-tuple-element.31), channel_id=1, source_target_pairs={{0,224},{32,0},{64,32},{96,64},{128,96},{160,128},{192,160},{224,1... | collective-permute-start | bytes 1179656 | tf_op jit(solution)/shard_map/ppermute | solution.py:26
  112.6 32.3 %collective-permute-start.26 = (bf16[1024,1024]{1,0:T(8,128)(2,1)S(1)}, bf16[1024,1024]{1,0:T(8,128)(2,1)S(1)}, u32[]{:S(2)}, u32[]{:S(2)}) collective-permute-start(bf16[1024,1024]{1,0:T(8,128)(2,1)S(1)} %shard_map.113), channel_id=1, source_target_pairs={{0,1},{1,0},{2,3},{3,2},{4,5},{5,4},{6,7},{7,6},{8,9},{9,8},{10,11... | collective-permute-start | bytes 6291464 | tf_op jit(solution)/shard_map/ppermute | solution.py:26
  114.7 30.2 %copy-start.4 = (bf16[768,1024]{1,0:T(8,128)(2,1)S(1)}, bf16[768,1024]{1,0:T(8,128)(2,1)}, u32[]{:S(2)}) copy-start(bf16[768,1024]{1,0:T(8,128)(2,1)} %copy-done.2) | copy-start | bytes 4718596
  114.7 12.4 %collective-permute-start.14 = (bf16[96,2048]{1,0:T(8,128)(2,1)S(1)}, bf16[96,2048]{1,0:T(8,128)(2,1)S(1)}, u32[]{:S(2)}, u32[]{:S(2)}) collective-permute-start(bf16[96,2048]{1,0:T(8,128)(2,1)S(1)} %get-tuple-element.58), channel_id=1, source_target_pairs={{0,32},{32,64},{64,96},{96,128},{128,160},{160,192},{192,224},{224... | collective-permute-start | bytes 1179656 | tf_op jit(solution)/shard_map/ppermute | solution.py:26
  115.6 18.1 %collective-permute-start.16 = (bf16[96,2048]{1,0:T(8,128)(2,1)S(1)}, bf16[96,2048]{1,0:T(8,128)(2,1)S(1)}, u32[]{:S(2)}, u32[]{:S(2)}) collective-permute-start(bf16[96,2048]{1,0:T(8,128)(2,1)S(1)} %get-tuple-element.59), channel_id=1, source_target_pairs={{0,224},{32,0},{64,32},{96,64},{128,96},{160,128},{192,160},{224,1... | collective-permute-start | bytes 1179656 | tf_op jit(solution)/shard_map/ppermute | solution.py:26
  116.9 19.7 %collective-permute-start.20 = (bf16[24,2048]{1,0:T(8,128)(2,1)S(1)}, bf16[24,2048]{1,0:T(8,128)(2,1)S(1)}, u32[]{:S(2)}, u32[]{:S(2)}) collective-permute-start(bf16[24,2048]{1,0:T(8,128)(2,1)S(1)} %get-tuple-element.63), channel_id=1, source_target_pairs={{0,128},{32,160},{64,192},{96,224},{128,0},{160,32},{192,64},{224,... | collective-permute-start | bytes 294920 | tf_op jit(solution)/shard_map/ppermute | solution.py:26
  118.6 20.3 %collective-permute-start.22 = (bf16[24,2048]{1,0:T(8,128)(2,1)S(1)}, bf16[24,2048]{1,0:T(8,128)(2,1)S(1)}, u32[]{:S(2)}, u32[]{:S(2)}) collective-permute-start(bf16[24,2048]{1,0:T(8,128)(2,1)S(1)} %get-tuple-element.64), channel_id=1, source_target_pairs={{0,160},{32,192},{64,224},{96,0},{128,32},{160,64},{192,96},{224,1... | collective-permute-start | bytes 294920 | tf_op jit(solution)/shard_map/ppermute | solution.py:26
  127.2 12.3 %collective-permute-start.21 = (bf16[24,2048]{1,0:T(8,128)(2,1)S(1)}, bf16[24,2048]{1,0:T(8,128)(2,1)S(1)}, u32[]{:S(2)}, u32[]{:S(2)}) collective-permute-start(bf16[24,2048]{1,0:T(8,128)(2,1)S(1)} %get-tuple-element.65), channel_id=1, source_target_pairs={{0,96},{32,128},{64,160},{96,192},{128,224},{160,0},{192,32},{224,... | collective-permute-start | bytes 294920 | tf_op jit(solution)/shard_map/ppermute | solution.py:26
  133.9 6.9 %collective-permute-start.23 = (bf16[24,2048]{1,0:T(8,128)(2,1)S(1)}, bf16[24,2048]{1,0:T(8,128)(2,1)S(1)}, u32[]{:S(2)}, u32[]{:S(2)}) collective-permute-start(bf16[24,2048]{1,0:T(8,128)(2,1)S(1)} %get-tuple-element.60), channel_id=1, source_target_pairs={{0,16},{8,24},{16,0},{24,8},{1,17},{9,25},{17,1},{25,9},{2,18},{10... | collective-permute-start | bytes 294920 | tf_op jit(solution)/shard_map/ppermute | solution.py:26
  136.6 4.6 %collective-permute-start.25 = (bf16[24,2048]{1,0:T(8,128)(2,1)S(1)}, bf16[24,2048]{1,0:T(8,128)(2,1)S(1)}, u32[]{:S(2)}, u32[]{:S(2)}) collective-permute-start(bf16[24,2048]{1,0:T(8,128)(2,1)S(1)} %get-tuple-element.61), channel_id=1, source_target_pairs={{0,24},{8,0},{16,8},{24,16},{1,25},{9,1},{17,9},{25,17},{2,26},{10... | collective-permute-start | bytes 294920 | tf_op jit(solution)/shard_map/ppermute | solution.py:26
  138.9 5.8 %collective-permute-start.24 = (bf16[24,2048]{1,0:T(8,128)(2,1)S(1)}, bf16[24,2048]{1,0:T(8,128)(2,1)S(1)}, u32[]{:S(2)}, u32[]{:S(2)}) collective-permute-start(bf16[24,2048]{1,0:T(8,128)(2,1)S(1)} %get-tuple-element.62), channel_id=1, source_target_pairs={{0,8},{8,16},{16,24},{24,0},{1,9},{9,17},{17,25},{25,1},{2,10},{10... | collective-permute-start | bytes 294920 | tf_op jit(solution)/shard_map/ppermute | solution.py:26
  147.3 16.4 %collective-permute-start.27 = (bf16[256,1024]{1,0:T(8,128)(2,1)S(1)}, bf16[256,1024]{1,0:T(8,128)(2,1)S(1)}, u32[]{:S(2)}, u32[]{:S(2)}) collective-permute-start(bf16[256,1024]{1,0:T(8,128)(2,1)S(1)} %get-tuple-element.38), channel_id=1, source_target_pairs={{0,4},{2,6},{4,0},{6,2},{1,5},{3,7},{5,1},{7,3},{8,12},{10,14},{12... | collective-permute-start | bytes 1572872 | tf_op jit(solution)/shard_map/ppermute | solution.py:26
  150.7 18.9 %collective-permute-start.28 = (bf16[256,1024]{1,0:T(8,128)(2,1)S(1)}, bf16[256,1024]{1,0:T(8,128)(2,1)S(1)}, u32[]{:S(2)}, u32[]{:S(2)}) collective-permute-start(bf16[256,1024]{1,0:T(8,128)(2,1)S(1)} %get-tuple-element.39), channel_id=1, source_target_pairs={{0,2},{2,4},{4,6},{6,0},{1,3},{3,5},{5,7},{7,1},{8,10},{10,12},{12... | collective-permute-start | bytes 1572872 | tf_op jit(solution)/shard_map/ppermute | solution.py:26
  151.3 18.7 %collective-permute-start.29 = (bf16[256,1024]{1,0:T(8,128)(2,1)S(1)}, bf16[256,1024]{1,0:T(8,128)(2,1)S(1)}, u32[]{:S(2)}, u32[]{:S(2)}) collective-permute-start(bf16[256,1024]{1,0:T(8,128)(2,1)S(1)} %get-tuple-element.40), channel_id=1, source_target_pairs={{0,6},{2,0},{4,2},{6,4},{1,7},{3,1},{5,3},{7,5},{8,14},{10,8},{12,... | collective-permute-start | bytes 1572872 | tf_op jit(solution)/shard_map/ppermute | solution.py:26
  (18 other events, 170.4 us)

commit v3 on v1

--- a/solution.py
+++ b/solution.py
@@ -121,67 +121,41 @@
     )(scores, matrix, order, vectors)
 
 
-def product_over_tokens(rows, grad):
+def vocab_product(rows, grad, first, share):
+    part = pl.ds(pl.multiple_of(first * share, share), share)
     return lax.dot_general(
-        rows[...], grad[...], (((0,), (0,)), ((), ())), preferred_element_type=f32
+        rows[:, part], grad[...], (((0,), (0,)), ((), ())), preferred_element_type=f32
     )
 
 
 def other_kernel(place, rows, grad, out):
-    out[...] = product_over_tokens(rows, grad).astype(bf16)
+    share = rows.shape[1] // (NY * NC)
+
+    def body(y, carry):
+        product = vocab_product(rows, grad, y * NC + 1 - place[1], share)
+        out[pl.ds(pl.multiple_of(y * share, share), share), :] = product.astype(bf16)
+        return carry
+
+    lax.fori_loop(0, NY, body, 0)
 
 
 def chip_kernel(place, rows, grad, other, own, *away):
-    product = product_over_tokens(rows, grad) + other[...].astype(f32)
+    share = rows.shape[1] // (NY * NC)
     for k, ref in enumerate((own, *away)):
-
-        @pl.when(pl.program_id(0) == NY - 1 - k)
-        def store(ref=ref):
-            ref[...] = product.astype(ref.dtype)
-
-
-def other_product(place, rows, grad):
-    share = rows.shape[1] // (NY * NC)
-    tokens, columns = grad.shape
-    return pl.pallas_call(
-        other_kernel,
-        out_shape=jax.ShapeDtypeStruct((NY * share, columns), bf16),
-        grid_spec=pltpu.PrefetchScalarGridSpec(
-            num_scalar_prefetch=1,
-            grid=(NY,),
-            in_specs=[
-                pl.BlockSpec((tokens, share), lambda y, place: (0, y * NC + 1 - place[1])),
-                pl.BlockSpec((tokens, columns), lambda y, place: (0, 0)),
-            ],
-            out_specs=pl.BlockSpec((share, columns), lambda y, place: (y, 0)),
-        ),
-    )(place, rows, grad)
-
-
-def chip_products(place, rows, grad, other):
-    share = rows.shape[1] // (NY * NC)
-    tokens, columns = grad.shape
-
-    def at(step, place):
-        return lax.rem(place[0] + NY - 1 - step, NY)
-
-    return pl.pallas_call(
-        chip_kernel,
-        out_shape=[jax.ShapeDtypeStruct((share, columns), f32)]
-        + [jax.ShapeDtypeStruct((share, columns), bf16)] * (NY - 1),
-        grid_spec=pltpu.PrefetchScalarGridSpec(
-            num_scalar_prefetch=1,
-            grid=(NY,),
-            in_specs=[
-                pl.BlockSpec(
-                    (tokens, share), lambda step, place: (0, at(step, place) * NC + place[1])
-                ),
-                pl.BlockSpec((tokens, columns), lambda step, place: (0, 0)),
-                pl.BlockSpec((share, columns), lambda step, place: (at(step, place), 0)),
-            ],
-            out_specs=[pl.BlockSpec((share, columns), lambda step, place: (0, 0))] * NY,
-        ),
-    )(place, rows, grad, other)
+        y = lax.rem(place[0] + k, NY)
+        product = vocab_product(rows, grad, y * NC + place[1], share)
+        product = product + other[pl.ds(pl.multiple_of(y * share, share), share), :].astype(f32)
+        ref[...] = product.astype(ref.dtype)
+
+
+def shaped(*shapes):
+    return tuple(jax.ShapeDtypeStruct(dims, kind) for dims, kind in shapes)
+
+
+def spaces(scalars, arrays):
+    return [pl.BlockSpec(memory_space=pltpu.SMEM)] * scalars + [
+        pl.BlockSpec(memory_space=pltpu.VMEM)
+    ] * arrays
 
 
 def whole(hidden_rows, norm_gain, vocab_matrix, vocab_bias, targets, loss_weight):
@@ -189,7 +163,7 @@
     inverse_rms = lax.rsqrt(jnp.mean(inputs * inputs, axis=-1, keepdims=True) + epsilon)
     unit_rows = inputs * inverse_rms
     normed = (unit_rows * norm_gain).astype(bf16)
-    own, _ = normed.shape
+    own, width = normed.shape
     total_rows = own * NZ * NX
     columns = vocab_matrix.shape[1]
 
@@ -202,10 +176,6 @@
     threes = {kx: taken_from(three, "vp_1", kx) for kx in (2, 1, 3)}
     up2 = taken_from(up1, "vp_0", 1)
     down2 = taken_from(down1, "vp_0", -1)
-    rows_all = jnp.concatenate(
-        [line, up1, down1, three] + [threes[kx] for kx in range(1, NX)] + [up2, down2]
-    )
-
     place_z, place_x = lax.axis_index("vp_0"), lax.axis_index("vp_1")
     place = slots(own)
     owner = (place_z + place[:, 0]) % NZ * NX + (place_x + place[:, 1]) % NX
@@ -217,6 +187,9 @@
         order, [targets[:, 0].astype(f32), loss_weight[:, 0]], (1,)
     )
     target_col = target_col.astype(jnp.int32) - lax.axis_index(VP) * columns
+    *early, target_col = lax.optimization_barrier((line, up1, down1, three, target_col))
+    late = [threes[kx] for kx in range(1, NX)] + [up2, down2]
+    rows_all = jnp.concatenate(early + late)
     column_ids = lax.broadcasted_iota(jnp.int32, (total_rows, columns), 1)
     is_target = column_ids == target_col[:, None]
 
@@ -255,10 +228,23 @@
     from_above = sent_to(downward, "vp_0", -1)
     far_x = {kx: sent_to(far_away[kx - 1], "vp_1", kx) for kx in (2, 1, 3)}
 
+    share = width // (NY * NC)
     place = jnp.stack([lax.axis_index("dp_0"), lax.axis_index("dp_1")])
-    other = other_product(place, rows_all, score_grad)
+    (other,) = pl.pallas_call(
+    other_kernel,
+    out_shape=shaped(((NY * share, columns), bf16)),
+    in_specs=spaces(1, 2),
+    out_specs=spaces(0, 1),
+    )(place, rows_all, score_grad)
     other = taken_from(other, "dp_1", 1)
-    vocab_grad, *away = chip_products(place, rows_all, score_grad, other)
+    vocab_grad, *away = pl.pallas_call(
+    chip_kernel,
+    out_shape=shaped(
+        ((share, columns), f32), *[((share, columns), bf16)] * (NY - 1)
+    ),
+    in_specs=spaces(1, 3),
+    out_specs=spaces(0, NY),
+    )(place, rows_all, score_grad, other)
     chip_y = {k: sent_to(away[k - 1], "dp_0", k) for k in (2, 1, 3)}
     above, below = near[block : 2 * block], near[2 * block :]
     from_below = sent_to((above + from_below.astype(f32)).astype(bf16), "vp_0", 1)

time: 170 us -> 165 us (0.971)
  other arithmetic: 16 us -> 13.5 us
  transfers between devices with their start and end apart: 31 -> 31, of which waited for: 9 -> 12; matrix products, arithmetic and copies ran while one was open for 8% -> 5% of each run, Pallas kernels for 4% -> 4%
where the time goes in v3:
time: 165 us; the launch traced here: 164 us
  waiting for transfers between devices  62.4 us (38%)
  starting transfers between devices  55.6 us (34%)
  Pallas kernels  22.4 us (14%)
  other arithmetic  13.5 us (8%)
  matrix products  4.66 us (3%)
  local copies, waits for them, and re-layouts  3.92 us (2%)
    ppermute x30, waiting for transfers between devices, taken_from(): lax.ppermute(array, axis, [(i, (i - step) % count) for i in range(count)])  51.9 us
    ppermute x30, starting transfers between devices, taken_from(): lax.ppermute(array, axis, [(i, (i - step) % count) for i in range(count)])  50.9 us
    all_to_all x1, waiting for transfers between devices, whole(): lax.all_to_all(packed, VP, split_axis=0, concat_axis=0, tiled=True)[:, 0]  10.5 us
    pallas_call x1, Pallas kernels, gradients(): pl.pallas_call(gradient_kernel, grid=(width // step,), out_shape=[jax.Sha...  10.3 us
    pallas_call x1, Pallas kernels, whole(): pl.pallas_call(other_kernel, out_shape=shaped(((NY * share, columns), bf1...  6.36 us
    pallas_call x1, Pallas kernels, whole(): pl.pallas_call(chip_kernel, out_shape=shaped(((share, columns), f32), *[(...  5.72 us
    all_to_all x1, starting transfers between devices, whole(): lax.all_to_all(packed, VP, split_axis=0, concat_axis=0, tiled=True)[:, 0]  4.7 us
    dot_general x1, matrix products, whole(): jnp.dot(rows_all, vocab_matrix, preferred_element_type=f32)  3.51 us
  transfers between devices with their start and end apart: 31, of which 12 were waited for; matrix products, arithmetic and copies ran while one was open for 5% of the time, Pallas kernels for 4%

profile of v3, /device:TPU:8, one launch (start us, length us, event | category | flops | bytes accessed | tf_op | source)
XLA Modules:
  0.0 163.5 jit_solution(12512193479163183057)
XLA Ops:
  2.7 4.7 %collective-permute-start.7 = (bf16[24,2048]{1,0:T(8,128)(2,1)S(1)}, bf16[24,2048]{1,0:T(8,128)(2,1)S(1)}, u32[]{:S(2)}, u32[]{:S(2)}) collective-permute-start(bf16[24,2048]{1,0:T(8,128)(2,1)S(1)} %fusion.8), channel_id=1, source_target_pairs={{0,96},{32,128},{64,160},{96,192},{128,224},{160,0},{192,32},{224,... | collective-permute-start | bytes 294920 | tf_op jit(solution)/shard_map/ppermute | solution.py:26
  7.4 4.5 %collective-permute-start.6 = (bf16[24,2048]{1,0:T(8,128)(2,1)S(1)}, bf16[24,2048]{1,0:T(8,128)(2,1)S(1)}, u32[]{:S(2)}, u32[]{:S(2)}) collective-permute-start(bf16[24,2048]{1,0:T(8,128)(2,1)S(1)} %fusion.8), channel_id=1, source_target_pairs={{0,128},{32,160},{64,192},{96,224},{128,0},{160,32},{192,64},{224,... | collective-permute-start | bytes 294920 | tf_op jit(solution)/shard_map/ppermute | solution.py:26
  11.9 1.5 collective-permute-start.2
  13.3 2.7 %collective-permute-start.1 = (bf16[24,2048]{1,0:T(8,128)(2,1)S(1)}, bf16[24,2048]{1,0:T(8,128)(2,1)S(1)}, u32[]{:S(2)}, u32[]{:S(2)}) collective-permute-start(bf16[24,2048]{1,0:T(8,128)(2,1)S(1)} %fusion.8), channel_id=1, source_target_pairs={{0,16},{8,24},{16,0},{24,8},{1,17},{9,25},{17,1},{25,9},{2,18},{10... | collective-permute-start | bytes 294920 | tf_op jit(solution)/shard_map/ppermute | solution.py:26
  20.4 3.2 %collective-permute-start.5 = (bf16[24,2048]{1,0:T(8,128)(2,1)S(1)}, bf16[24,2048]{1,0:T(8,128)(2,1)S(1)}, u32[]{:S(2)}, u32[]{:S(2)}) collective-permute-start(bf16[24,2048]{1,0:T(8,128)(2,1)S(1)} %fusion.8), channel_id=1, source_target_pairs={{0,160},{32,192},{64,224},{96,0},{128,32},{160,64},{192,96},{224,1... | collective-permute-start | bytes 294920 | tf_op jit(solution)/shard_map/ppermute | solution.py:26
  24.7 2.2 %collective-permute-start.3 = (bf16[96,2048]{1,0:T(8,128)(2,1)S(1)}, bf16[96,2048]{1,0:T(8,128)(2,1)S(1)}, u32[]{:S(2)}, u32[]{:S(2)}) collective-permute-start(bf16[96,2048]{1,0:T(8,128)(2,1)S(1)} %pad_maximum_fusion), channel_id=1, source_target_pairs={{0,224},{32,0},{64,32},{96,64},{128,96},{160,128},{192,160},{224,1... | collective-permute-start | bytes 1179656 | tf_op jit(solution)/shard_map/ppermute | solution.py:26
  27.6 2.3 %collective-permute-done.5 = bf16[24,2048]{1,0:T(8,128)(2,1)S(1)} collective-permute-done((bf16[24,2048]{1,0:T(8,128)(2,1)S(1)}, bf16[24,2048]{1,0:T(8,128)(2,1)S(1)}, u32[]{:S(2)}, u32[]{:S(2)}) %collective-permute-start.5) | collective-permute-done | bytes 98336 | tf_op jit(solution)/shard_map/ppermute | solution.py:26
  31.6 1.9 %collective-permute-start.8 = (bf16[72,2048]{1,0:T(8,128)(2,1)S(1)}, bf16[72,2048]{1,0:T(8,128)(2,1)S(1)}, u32[]{:S(2)}, u32[]{:S(2)}) collective-permute-start(bf16[72,2048]{1,0:T(8,128)(2,1)S(1)} %pad_maximum_fusion.1), channel_id=1, source_target_pairs={{0,24},{8,0},{16,8},{24,16},{1,25},{9,1},{17,9},{25,17},{2,26},{10... | collective-permute-start | bytes 884744 | tf_op jit(solution)/shard_map/ppermute | solution.py:26
  34.1 4.1 %collective-permute-done.3 = bf16[96,2048]{1,0:T(8,128)(2,1)S(1)} collective-permute-done((bf16[96,2048]{1,0:T(8,128)(2,1)S(1)}, bf16[96,2048]{1,0:T(8,128)(2,1)S(1)}, u32[]{:S(2)}, u32[]{:S(2)}) %collective-permute-start.3) | collective-permute-done | bytes 393248 | tf_op jit(solution)/shard_map/ppermute | solution.py:26
  38.8 2.8 %collective-permute-start.11 = (bf16[96,2048]{1,0:T(8,128)(2,1)S(1)}, bf16[96,2048]{1,0:T(8,128)(2,1)S(1)}, u32[]{:S(2)}, u32[]{:S(2)}) collective-permute-start(bf16[96,2048]{1,0:T(8,128)(2,1)S(1)} %collective-permute-done.3), channel_id=1, source_target_pairs={{0,224},{32,0},{64,32},{96,64},{128,96},{160,128},{192,160},{224,1... | collective-permute-start | bytes 1179656 | tf_op jit(solution)/shard_map/ppermute | solution.py:26
  41.6 2.3 %collective-permute-done.8 = bf16[72,2048]{1,0:T(8,128)(2,1)S(1)} collective-permute-done((bf16[72,2048]{1,0:T(8,128)(2,1)S(1)}, bf16[72,2048]{1,0:T(8,128)(2,1)S(1)}, u32[]{:S(2)}, u32[]{:S(2)}) %collective-permute-start.8) | collective-permute-done | bytes 294944 | tf_op jit(solution)/shard_map/ppermute | solution.py:26
  44.0 5.0 %collective-permute-done.11 = bf16[96,2048]{1,0:T(8,128)(2,1)S(1)} collective-permute-done((bf16[96,2048]{1,0:T(8,128)(2,1)S(1)}, bf16[96,2048]{1,0:T(8,128)(2,1)S(1)}, u32[]{:S(2)}, u32[]{:S(2)}) %collective-permute-start.11) | collective-permute-done | bytes 393248 | tf_op jit(solution)/shard_map/ppermute | solution.py:26
  49.5 3.5 %fusion.41 = (f32[768]{0:T(1024)S(1)}, f32[768,1024]{1,0:T(8,128)S(1)}) fusion(f32[1024]{0:T(1024)S(1)} %copy-done.9, bf16[768,2048]{1,0:T(8,128)(2,1)S(1)} %constant_dynamic-update-slice_fusion.rows, bf16[2048,1024]{1,0:T(8,128)(2,1)S(1)} %copy-done.2), kind=kOutput, calls=%fused_computation.110 | convolution fusion | flops 3222797568 | bytes 10492928 | tf_op jit(solution)/shard_map/dot_general | solution.py:196
  53.1 1.7 %copy-done.1 = f32[768,1024]{1,0:T(8,128)} copy-done((f32[768,1024]{1,0:T(8,128)}, f32[768,1024]{1,0:T(8,128)S(1)}, u32[]{:S(2)}) %copy-start.1) | copy-done | bytes 3145752
  57.5 4.7 %all-to-all-start = ((f32[32,1,896]{2,1,0:T(1,128)}), f32[32,1,896]{2,1,0:T(1,128)S(1)}, u32[]{:S(2)}, u32[]{:S(2)}) async-start(f32[32,1,896]{2,1,0:T(1,128)} %broadcast_in_dim.16), calls=%async_computation | async-start | bytes 229376 | tf_op jit(solution)/shard_map/all_to_all | solution.py:206
  62.2 10.5 %all-to-all-done = f32[32,1,896]{2,1,0:T(1,128)S(1)} async-done(((f32[32,1,896]{2,1,0:T(1,128)}), f32[32,1,896]{2,1,0:T(1,128)S(1)}, u32[]{:S(2)}, u32[]{:S(2)}) %all-to-all-start) | async-done | bytes 114720 | tf_op jit(solution)/shard_map/all_to_all | solution.py:206
  73.5 10.3 %shard_map.112 = (bf16[768,1024]{1,0:T(8,128)(2,1)}, f32[72,2048]{1,0:T(8,128)}, f32[288,2048]{1,0:T(8,128)}, bf16[96,2048]{1,0:T(8,128)(2,1)}, bf16[96,2048]{1,...) custom-call(f32[768,1024]{1,0:T(8,128)} %copy-done.1, ...), custom_call_target="tpu_custom_call" | custom-call | tf_op jit(solution)/shard_map/pallas_call | solution.py:108
  84.0 2.6 %collective-permute-start.18 = (bf16[72,2048]{1,0:T(8,128)(2,1)}, bf16[72,2048]{1,0:T(8,128)(2,1)}, u32[]{:S(2)}, u32[]{:S(2)}) collective-permute-start(bf16[72,2048]{1,0:T(8,128)(2,1)} %get-tuple-element.30), channel_id=1, source_target_pairs={{0,16},{8,24},{16,0},{24,8},{1,17},{9,25},{17,1},{25,9},{2,18},{10... | collective-permute-start | bytes 884744 | tf_op jit(solution)/shard_map/ppermute | solution.py:26
  88.8 2.7 %collective-permute-start.15 = (bf16[96,2048]{1,0:T(8,128)(2,1)}, bf16[96,2048]{1,0:T(8,128)(2,1)}, u32[]{:S(2)}, u32[]{:S(2)}) collective-permute-start(bf16[96,2048]{1,0:T(8,128)(2,1)} %get-tuple-element.27), channel_id=1, source_target_pairs={{0,224},{32,0},{64,32},{96,64},{128,96},{160,128},{192,160},{224,1... | collective-permute-start | bytes 1179656 | tf_op jit(solution)/shard_map/ppermute | solution.py:26
  91.5 6.4 %shard_map.113 = bf16[1024,1024]{1,0:T(8,128)(2,1)} custom-call(s32[2]{0:T(128)} %pad_add_fusion.place, bf16[768,2048]{1,0:T(8,128)(2,1)} %copy-done, bf16[768,1024]{1,0:T(8,128)(2,1)} %get-tuple-element.32.grad), custom_call_target="tpu_custom_call" | custom-call | tf_op jit(solution)/shard_map/pallas_call | solution.py:233
  100.9 3.1 %collective-permute-start.16 = (bf16[96,2048]{1,0:T(8,128)(2,1)S(1)}, bf16[96,2048]{1,0:T(8,128)(2,1)S(1)}, u32[]{:S(2)}, u32[]{:S(2)}) collective-permute-start(bf16[96,2048]{1,0:T(8,128)(2,1)S(1)} %get-tuple-element.55), channel_id=1, source_target_pairs={{0,224},{32,0},{64,32},{96,64},{128,96},{160,128},{192,160},{224,1... | collective-permute-start | bytes 1179656 | tf_op jit(solution)/shard_map/ppermute | solution.py:26
  105.3 2.3 %collective-permute-start.22 = (bf16[24,2048]{1,0:T(8,128)(2,1)S(1)}, bf16[24,2048]{1,0:T(8,128)(2,1)S(1)}, u32[]{:S(2)}, u32[]{:S(2)}) collective-permute-start(bf16[24,2048]{1,0:T(8,128)(2,1)S(1)} %get-tuple-element.60), channel_id=1, source_target_pairs={{0,160},{32,192},{64,224},{96,0},{128,32},{160,64},{192,96},{224,1... | collective-permute-start | bytes 294920 | tf_op jit(solution)/shard_map/ppermute | solution.py:26
  107.6 12.8 %collective-permute-done.14 = bf16[96,2048]{1,0:T(8,128)(2,1)S(1)} collective-permute-done((bf16[96,2048]{1,0:T(8,128)(2,1)S(1)}, bf16[96,2048]{1,0:T(8,128)(2,1)S(1)}, u32[]{:S(2)}, u32[]{:S(2)}) %collective-permute-start.14) | collective-permute-done | bytes 393248 | tf_op jit(solution)/shard_map/ppermute | solution.py:26
  120.5 2.3 %collective-permute-start.23 = (bf16[24,2048]{1,0:T(8,128)(2,1)S(1)}, bf16[24,2048]{1,0:T(8,128)(2,1)S(1)}, u32[]{:S(2)}, u32[]{:S(2)}) collective-permute-start(bf16[24,2048]{1,0:T(8,128)(2,1)S(1)} %get-tuple-element.56), channel_id=1, source_target_pairs={{0,16},{8,24},{16,0},{24,8},{1,17},{9,25},{17,1},{25,9},{2,18},{10... | collective-permute-start | bytes 294920 | tf_op jit(solution)/shard_map/ppermute | solution.py:26
  125.4 2.5 %collective-permute-done.21 = bf16[24,2048]{1,0:T(8,128)(2,1)S(1)} collective-permute-done((bf16[24,2048]{1,0:T(8,128)(2,1)S(1)}, bf16[24,2048]{1,0:T(8,128)(2,1)S(1)}, u32[]{:S(2)}, u32[]{:S(2)}) %collective-permute-start.21) | collective-permute-done | bytes 98336 | tf_op jit(solution)/shard_map/ppermute | solution.py:26
  128.0 2.1 %collective-permute-done.24 = bf16[24,2048]{1,0:T(8,128)(2,1)S(1)} collective-permute-done((bf16[24,2048]{1,0:T(8,128)(2,1)S(1)}, bf16[24,2048]{1,0:T(8,128)(2,1)S(1)}, u32[]{:S(2)}, u32[]{:S(2)}) %collective-permute-start.24) | collective-permute-done | bytes 98336 | tf_op jit(solution)/shard_map/ppermute | solution.py:26
  130.3 5.7 %shard_map.114 = (f32[256,1024]{1,0:T(8,128)}, bf16[256,1024]{1,0:T(8,128)(2,1)}, bf16[256,1024]{1,0:T(8,128)(2,1)}, bf16[256,1024]{1,0:T(8,128)(2,1)}) custom-call(s32[2]{0:T(128)} %pad_add_fusion.place, bf16[768,2048]{1,0:T(8,128)(2,1)} %copy-done, bf16[768,1024]{1,0:T(8,128)(2,1)} %get-tuple-element.32.grad, bf16[1024,1024]{1,0:T(8,128)(2,1)} %collective-permute-done.26.other), custom_call_target="tpu_custom_call" | custom-call | tf_op jit(solution)/shard_map/pallas_call | solution.py:240
  136.1 2.3 %collective-permute-start.27 = (bf16[256,1024]{1,0:T(8,128)(2,1)}, bf16[256,1024]{1,0:T(8,128)(2,1)S(1)}, u32[]{:S(2)}, u32[]{:S(2)}) collective-permute-start(bf16[256,1024]{1,0:T(8,128)(2,1)} %get-tuple-element.34), channel_id=1, source_target_pairs={{0,4},{2,6},{4,0},{6,2},{1,5},{3,7},{5,1},{7,3},{8,12},{10,14},{12... | collective-permute-start | bytes 1572872 | tf_op jit(solution)/shard_map/ppermute | solution.py:26
  138.4 2.0 %collective-permute-start.29 = (bf16[256,1024]{1,0:T(8,128)(2,1)}, bf16[256,1024]{1,0:T(8,128)(2,1)S(1)}, u32[]{:S(2)}, u32[]{:S(2)}) collective-permute-start(bf16[256,1024]{1,0:T(8,128)(2,1)} %get-tuple-element.36), channel_id=1, source_target_pairs={{0,6},{2,0},{4,2},{6,4},{1,7},{3,1},{5,3},{7,5},{8,14},{10,8},{12,... | collective-permute-start | bytes 1572872 | tf_op jit(solution)/shard_map/ppermute | solution.py:26
  141.4 11.2 %collective-permute-done.27 = bf16[256,1024]{1,0:T(8,128)(2,1)S(1)} collective-permute-done((bf16[256,1024]{1,0:T(8,128)(2,1)}, bf16[256,1024]{1,0:T(8,128)(2,1)S(1)}, u32[]{:S(2)}, u32[]{:S(2)}) %collective-permute-start.27) | collective-permute-done | bytes 524320 | tf_op jit(solution)/shard_map/ppermute | solution.py:26
  152.6 8.4 %collective-permute-done.28 = bf16[256,1024]{1,0:T(8,128)(2,1)S(1)} collective-permute-done((bf16[256,1024]{1,0:T(8,128)(2,1)}, bf16[256,1024]{1,0:T(8,128)(2,1)S(1)}, u32[]{:S(2)}, u32[]{:S(2)}) %collective-permute-start.28) | collective-permute-done | bytes 524320 | tf_op jit(solution)/shard_map/ppermute | solution.py:26
  161.0 2.5 %convert_add_fusion = f32[256,1024]{1,0:T(8,128)} fusion(bf16[256,1024]{1,0:T(8,128)(2,1)S(1)} %collective-permute-done.29, bf16[256,1024]{1,0:T(8,128)(2,1)S(1)} %collective-permute-done.28, f32[256,1024]{1,0:T(8,128)} %get-tuple-element.33, bf16[256,1024]{1,0:T(8,128)(2,1)S(1)} %collective-permute-done.27), kind=kLoop, calls=%fused_computation.10 | loop fusion | flops 1572864 | bytes 3670016 | tf_op jit(solution)/shard_map/add | solution.py:269
  (107 shorter events, 25.5 us)
Async XLA Ops:
  2.7 25.0 %collective-permute-start.7 = (bf16[24,2048]{1,0:T(8,128)(2,1)S(1)}, bf16[24,2048]{1,0:T(8,128)(2,1)S(1)}, u32[]{:S(2)}, u32[]{:S(2)}) collective-permute-start(bf16[24,2048]{1,0:T(8,128)(2,1)S(1)} %fusion.8), channel_id=1, source_target_pairs={{0,96},{32,128},{64,160},{96,192},{128,224},{160,0},{192,32},{224,... | collective-permute-start | bytes 294920 | tf_op jit(solution)/shard_map/ppermute | solution.py:26
  7.4 20.3 %collective-permute-start.6 = (bf16[24,2048]{1,0:T(8,128)(2,1)S(1)}, bf16[24,2048]{1,0:T(8,128)(2,1)S(1)}, u32[]{:S(2)}, u32[]{:S(2)}) collective-permute-start(bf16[24,2048]{1,0:T(8,128)(2,1)S(1)} %fusion.8), channel_id=1, source_target_pairs={{0,128},{32,160},{64,192},{96,224},{128,0},{160,32},{192,64},{224,... | collective-permute-start | bytes 294920 | tf_op jit(solution)/shard_map/ppermute | solution.py:26
  11.9 8.5 %collective-permute-start.2 = (bf16[24,2048]{1,0:T(8,128)(2,1)S(1)}, bf16[24,2048]{1,0:T(8,128)(2,1)S(1)}, u32[]{:S(2)}, u32[]{:S(2)}) collective-permute-start(bf16[24,2048]{1,0:T(8,128)(2,1)S(1)} %fusion.8), channel_id=1, source_target_pairs={{0,8},{8,16},{16,24},{24,0},{1,9},{9,17},{17,25},{25,1},{2,10},{10... | collective-permute-start | bytes 294920 | tf_op jit(solution)/shard_map/ppermute | solution.py:26
  13.3 10.2 %collective-permute-start.1 = (bf16[24,2048]{1,0:T(8,128)(2,1)S(1)}, bf16[24,2048]{1,0:T(8,128)(2,1)S(1)}, u32[]{:S(2)}, u32[]{:S(2)}) collective-permute-start(bf16[24,2048]{1,0:T(8,128)(2,1)S(1)} %fusion.8), channel_id=1, source_target_pairs={{0,16},{8,24},{16,0},{24,8},{1,17},{9,25},{17,1},{25,9},{2,18},{10... | collective-permute-start | bytes 294920 | tf_op jit(solution)/shard_map/ppermute | solution.py:26
  16.1 7.5 %collective-permute-start = (bf16[24,2048]{1,0:T(8,128)(2,1)S(1)}, bf16[24,2048]{1,0:T(8,128)(2,1)S(1)}, u32[]{:S(2)}, u32[]{:S(2)}) collective-permute-start(bf16[24,2048]{1,0:T(8,128)(2,1)S(1)} %fusion.8), channel_id=1, source_target_pairs={{0,24},{8,0},{16,8},{24,16},{1,25},{9,1},{17,9},{25,17},{2,26},{10... | collective-permute-start | bytes 294920 | tf_op jit(solution)/shard_map/ppermute | solution.py:26
  20.4 9.6 %collective-permute-start.5 = (bf16[24,2048]{1,0:T(8,128)(2,1)S(1)}, bf16[24,2048]{1,0:T(8,128)(2,1)S(1)}, u32[]{:S(2)}, u32[]{:S(2)}) collective-permute-start(bf16[24,2048]{1,0:T(8,128)(2,1)S(1)} %fusion.8), channel_id=1, source_target_pairs={{0,160},{32,192},{64,224},{96,0},{128,32},{160,64},{192,96},{224,1... | collective-permute-start | bytes 294920 | tf_op jit(solution)/shard_map/ppermute | solution.py:26
  23.6 10.5 %collective-permute-start.4 = (bf16[96,2048]{1,0:T(8,128)(2,1)S(1)}, bf16[96,2048]{1,0:T(8,128)(2,1)S(1)}, u32[]{:S(2)}, u32[]{:S(2)}) collective-permute-start(bf16[96,2048]{1,0:T(8,128)(2,1)S(1)} %pad_maximum_fusion), channel_id=1, source_target_pairs={{0,32},{32,64},{64,96},{96,128},{128,160},{160,192},{192,224},{224... | collective-permute-start | bytes 1179656 | tf_op jit(solution)/shard_map/ppermute | solution.py:26
  24.7 13.5 %collective-permute-start.3 = (bf16[96,2048]{1,0:T(8,128)(2,1)S(1)}, bf16[96,2048]{1,0:T(8,128)(2,1)S(1)}, u32[]{:S(2)}, u32[]{:S(2)}) collective-permute-start(bf16[96,2048]{1,0:T(8,128)(2,1)S(1)} %pad_maximum_fusion), channel_id=1, source_target_pairs={{0,224},{32,0},{64,32},{96,64},{128,96},{160,128},{192,160},{224,1... | collective-permute-start | bytes 1179656 | tf_op jit(solution)/shard_map/ppermute | solution.py:26
  30.0 14.0 %collective-permute-start.10 = (bf16[72,2048]{1,0:T(8,128)(2,1)S(1)}, bf16[72,2048]{1,0:T(8,128)(2,1)S(1)}, u32[]{:S(2)}, u32[]{:S(2)}) collective-permute-start(bf16[72,2048]{1,0:T(8,128)(2,1)S(1)} %pad_maximum_fusion.1), channel_id=1, source_target_pairs={{0,8},{8,16},{16,24},{24,0},{1,9},{9,17},{17,25},{25,1},{2,10},{10... | collective-permute-start | bytes 884744 | tf_op jit(solution)/shard_map/ppermute | solution.py:26
  30.7 13.3 %collective-permute-start.9 = (bf16[72,2048]{1,0:T(8,128)(2,1)S(1)}, bf16[72,2048]{1,0:T(8,128)(2,1)S(1)}, u32[]{:S(2)}, u32[]{:S(2)}) collective-permute-start(bf16[72,2048]{1,0:T(8,128)(2,1)S(1)} %pad_maximum_fusion.1), channel_id=1, source_target_pairs={{0,16},{8,24},{16,0},{24,8},{1,17},{9,25},{17,1},{25,9},{2,18},{10... | collective-permute-start | bytes 884744 | tf_op jit(solution)/shard_map/ppermute | solution.py:26
  31.6 12.4 %collective-permute-start.8 = (bf16[72,2048]{1,0:T(8,128)(2,1)S(1)}, bf16[72,2048]{1,0:T(8,128)(2,1)S(1)}, u32[]{:S(2)}, u32[]{:S(2)}) collective-permute-start(bf16[72,2048]{1,0:T(8,128)(2,1)S(1)} %pad_maximum_fusion.1), channel_id=1, source_target_pairs={{0,24},{8,0},{16,8},{24,16},{1,25},{9,1},{17,9},{25,17},{2,26},{10... | collective-permute-start | bytes 884744 | tf_op jit(solution)/shard_map/ppermute | solution.py:26
  38.3 11.2 %collective-permute-start.12 = (bf16[96,2048]{1,0:T(8,128)(2,1)S(1)}, bf16[96,2048]{1,0:T(8,128)(2,1)S(1)}, u32[]{:S(2)}, u32[]{:S(2)}) collective-permute-start(bf16[96,2048]{1,0:T(8,128)(2,1)S(1)} %collective-permute-done.4), channel_id=1, source_target_pairs={{0,32},{32,64},{64,96},{96,128},{128,160},{160,192},{192,224},{224... | collective-permute-start | bytes 1179656 | tf_op jit(solution)/shard_map/ppermute | solution.py:26
  38.8 10.2 %collective-permute-start.11 = (bf16[96,2048]{1,0:T(8,128)(2,1)S(1)}, bf16[96,2048]{1,0:T(8,128)(2,1)S(1)}, u32[]{:S(2)}, u32[]{:S(2)}) collective-permute-start(bf16[96,2048]{1,0:T(8,128)(2,1)S(1)} %collective-permute-done.3), channel_id=1, source_target_pairs={{0,224},{32,0},{64,32},{96,64},{128,96},{160,128},{192,160},{224,1... | collective-permute-start | bytes 1179656 | tf_op jit(solution)/shard_map/ppermute | solution.py:26
  57.5 15.2 %all-to-all-start = ((f32[32,1,896]{2,1,0:T(1,128)}), f32[32,1,896]{2,1,0:T(1,128)S(1)}, u32[]{:S(2)}, u32[]{:S(2)}) async-start(f32[32,1,896]{2,1,0:T(1,128)} %broadcast_in_dim.16), calls=%async_computation | async-start | bytes 229376 | tf_op jit(solution)/shard_map/all_to_all | solution.py:206
  83.8 14.1 %collective-permute-start.17 = (bf16[72,2048]{1,0:T(8,128)(2,1)}, bf16[72,2048]{1,0:T(8,128)(2,1)}, u32[]{:S(2)}, u32[]{:S(2)}) collective-permute-start(bf16[72,2048]{1,0:T(8,128)(2,1)} %get-tuple-element.29), channel_id=1, source_target_pairs={{0,8},{8,16},{16,24},{24,0},{1,9},{9,17},{17,25},{25,1},{2,10},{10... | collective-permute-start | bytes 884744 | tf_op jit(solution)/shard_map/ppermute | solution.py:26
  84.0 14.2 %collective-permute-start.18 = (bf16[72,2048]{1,0:T(8,128)(2,1)}, bf16[72,2048]{1,0:T(8,128)(2,1)}, u32[]{:S(2)}, u32[]{:S(2)}) collective-permute-start(bf16[72,2048]{1,0:T(8,128)(2,1)} %get-tuple-element.30), channel_id=1, source_target_pairs={{0,16},{8,24},{16,0},{24,8},{1,17},{9,25},{17,1},{25,9},{2,18},{10... | collective-permute-start | bytes 884744 | tf_op jit(solution)/shard_map/ppermute | solution.py:26
  86.6 11.6 %collective-permute-start.19 = (bf16[72,2048]{1,0:T(8,128)(2,1)}, bf16[72,2048]{1,0:T(8,128)(2,1)}, u32[]{:S(2)}, u32[]{:S(2)}) collective-permute-start(bf16[72,2048]{1,0:T(8,128)(2,1)} %get-tuple-element.31), channel_id=1, source_target_pairs={{0,24},{8,0},{16,8},{24,16},{1,25},{9,1},{17,9},{25,17},{2,26},{10... | collective-permute-start | bytes 884744 | tf_op jit(solution)/shard_map/ppermute | solution.py:26
  88.2 11.3 %collective-permute-start.13 = (bf16[96,2048]{1,0:T(8,128)(2,1)}, bf16[96,2048]{1,0:T(8,128)(2,1)S(1)}, u32[]{:S(2)}, u32[]{:S(2)}) collective-permute-start(bf16[96,2048]{1,0:T(8,128)(2,1)} %get-tuple-element.26), channel_id=1, source_target_pairs={{0,32},{32,64},{64,96},{96,128},{128,160},{160,192},{192,224},{224... | collective-permute-start | bytes 1179656 | tf_op jit(solution)/shard_map/ppermute | solution.py:26
  88.8 10.7 %collective-permute-start.15 = (bf16[96,2048]{1,0:T(8,128)(2,1)}, bf16[96,2048]{1,0:T(8,128)(2,1)}, u32[]{:S(2)}, u32[]{:S(2)}) collective-permute-start(bf16[96,2048]{1,0:T(8,128)(2,1)} %get-tuple-element.27), channel_id=1, source_target_pairs={{0,224},{32,0},{64,32},{96,64},{128,96},{160,128},{192,160},{224,1... | collective-permute-start | bytes 1179656 | tf_op jit(solution)/shard_map/ppermute | solution.py:26
  97.9 32.5 %collective-permute-start.26 = (bf16[1024,1024]{1,0:T(8,128)(2,1)}, bf16[1024,1024]{1,0:T(8,128)(2,1)}, u32[]{:S(2)}, u32[]{:S(2)}) collective-permute-start(bf16[1024,1024]{1,0:T(8,128)(2,1)} %shard_map.113), channel_id=1, source_target_pairs={{0,1},{1,0},{2,3},{3,2},{4,5},{5,4},{6,7},{7,6},{8,9},{9,8},{10,11... | collective-permute-start | bytes 6291464 | tf_op jit(solution)/shard_map/ppermute | solution.py:26
  99.5 30.6 %copy-start.4 = (bf16[24,1,2048]{2,0,1:T(8,128)(2,1)S(1)}, bf16[24,1,2048]{2,0,1:T(8,128)(2,1)}, u32[]{:S(2)}) copy-start(bf16[24,1,2048]{2,0,1:T(8,128)(2,1)} %param.9) | copy-start | bytes 294916
  100.8 19.6 %collective-permute-start.14 = (bf16[96,2048]{1,0:T(8,128)(2,1)S(1)}, bf16[96,2048]{1,0:T(8,128)(2,1)S(1)}, u32[]{:S(2)}, u32[]{:S(2)}) collective-permute-start(bf16[96,2048]{1,0:T(8,128)(2,1)S(1)} %get-tuple-element.54), channel_id=1, source_target_pairs={{0,32},{32,64},{64,96},{96,128},{128,160},{160,192},{192,224},{224... | collective-permute-start | bytes 1179656 | tf_op jit(solution)/shard_map/ppermute | solution.py:26
  100.9 19.4 %collective-permute-start.16 = (bf16[96,2048]{1,0:T(8,128)(2,1)S(1)}, bf16[96,2048]{1,0:T(8,128)(2,1)S(1)}, u32[]{:S(2)}, u32[]{:S(2)}) collective-permute-start(bf16[96,2048]{1,0:T(8,128)(2,1)S(1)} %get-tuple-element.55), channel_id=1, source_target_pairs={{0,224},{32,0},{64,32},{96,64},{128,96},{160,128},{192,160},{224,1... | collective-permute-start | bytes 1179656 | tf_op jit(solution)/shard_map/ppermute | solution.py:26
  104.1 18.7 %collective-permute-start.20 = (bf16[24,2048]{1,0:T(8,128)(2,1)S(1)}, bf16[24,2048]{1,0:T(8,128)(2,1)S(1)}, u32[]{:S(2)}, u32[]{:S(2)}) collective-permute-start(bf16[24,2048]{1,0:T(8,128)(2,1)S(1)} %get-tuple-element.59), channel_id=1, source_target_pairs={{0,128},{32,160},{64,192},{96,224},{128,0},{160,32},{192,64},{224,... | collective-permute-start | bytes 294920 | tf_op jit(solution)/shard_map/ppermute | solution.py:26
  105.3 19.0 %collective-permute-start.22 = (bf16[24,2048]{1,0:T(8,128)(2,1)S(1)}, bf16[24,2048]{1,0:T(8,128)(2,1)S(1)}, u32[]{:S(2)}, u32[]{:S(2)}) collective-permute-start(bf16[24,2048]{1,0:T(8,128)(2,1)S(1)} %get-tuple-element.60), channel_id=1, source_target_pairs={{0,160},{32,192},{64,224},{96,0},{128,32},{160,64},{192,96},{224,1... | collective-permute-start | bytes 294920 | tf_op jit(solution)/shard_map/ppermute | solution.py:26
  120.4 7.6 %collective-permute-start.21 = (bf16[24,2048]{1,0:T(8,128)(2,1)S(1)}, bf16[24,2048]{1,0:T(8,128)(2,1)S(1)}, u32[]{:S(2)}, u32[]{:S(2)}) collective-permute-start(bf16[24,2048]{1,0:T(8,128)(2,1)S(1)} %get-tuple-element.61), channel_id=1, source_target_pairs={{0,96},{32,128},{64,160},{96,192},{128,224},{160,0},{192,32},{224,... | collective-permute-start | bytes 294920 | tf_op jit(solution)/shard_map/ppermute | solution.py:26
  120.5 7.4 %collective-permute-start.23 = (bf16[24,2048]{1,0:T(8,128)(2,1)S(1)}, bf16[24,2048]{1,0:T(8,128)(2,1)S(1)}, u32[]{:S(2)}, u32[]{:S(2)}) collective-permute-start(bf16[24,2048]{1,0:T(8,128)(2,1)S(1)} %get-tuple-element.56), channel_id=1, source_target_pairs={{0,16},{8,24},{16,0},{24,8},{1,17},{9,25},{17,1},{25,9},{2,18},{10... | collective-permute-start | bytes 294920 | tf_op jit(solution)/shard_map/ppermute | solution.py:26
  122.8 5.2 %collective-permute-start.25 = (bf16[24,2048]{1,0:T(8,128)(2,1)S(1)}, bf16[24,2048]{1,0:T(8,128)(2,1)S(1)}, u32[]{:S(2)}, u32[]{:S(2)}) collective-permute-start(bf16[24,2048]{1,0:T(8,128)(2,1)S(1)} %get-tuple-element.57), channel_id=1, source_target_pairs={{0,24},{8,0},{16,8},{24,16},{1,25},{9,1},{17,9},{25,17},{2,26},{10... | collective-permute-start | bytes 294920 | tf_op jit(solution)/shard_map/ppermute | solution.py:26
  124.3 5.8 %collective-permute-start.24 = (bf16[24,2048]{1,0:T(8,128)(2,1)S(1)}, bf16[24,2048]{1,0:T(8,128)(2,1)S(1)}, u32[]{:S(2)}, u32[]{:S(2)}) collective-permute-start(bf16[24,2048]{1,0:T(8,128)(2,1)S(1)} %get-tuple-element.58), channel_id=1, source_target_pairs={{0,8},{8,16},{16,24},{24,0},{1,9},{9,17},{17,25},{25,1},{2,10},{10... | collective-permute-start | bytes 294920 | tf_op jit(solution)/shard_map/ppermute | solution.py:26
  136.1 16.5 %collective-permute-start.27 = (bf16[256,1024]{1,0:T(8,128)(2,1)}, bf16[256,1024]{1,0:T(8,128)(2,1)S(1)}, u32[]{:S(2)}, u32[]{:S(2)}) collective-permute-start(bf16[256,1024]{1,0:T(8,128)(2,1)} %get-tuple-element.34), channel_id=1, source_target_pairs={{0,4},{2,6},{4,0},{6,2},{1,5},{3,7},{5,1},{7,3},{8,12},{10,14},{12... | collective-permute-start | bytes 1572872 | tf_op jit(solution)/shard_map/ppermute | solution.py:26
  138.4 22.6 %collective-permute-start.28 = (bf16[256,1024]{1,0:T(8,128)(2,1)}, bf16[256,1024]{1,0:T(8,128)(2,1)S(1)}, u32[]{:S(2)}, u32[]{:S(2)}) collective-permute-start(bf16[256,1024]{1,0:T(8,128)(2,1)} %get-tuple-element.35), channel_id=1, source_target_pairs={{0,2},{2,4},{4,6},{6,0},{1,3},{3,5},{5,7},{7,1},{8,10},{10,12},{12... | collective-permute-start | bytes 1572872 | tf_op jit(solution)/shard_map/ppermute | solution.py:26
  138.4 22.6 %collective-permute-start.29 = (bf16[256,1024]{1,0:T(8,128)(2,1)}, bf16[256,1024]{1,0:T(8,128)(2,1)S(1)}, u32[]{:S(2)}, u32[]{:S(2)}) collective-permute-start(bf16[256,1024]{1,0:T(8,128)(2,1)} %get-tuple-element.36), channel_id=1, source_target_pairs={{0,6},{2,0},{4,2},{6,4},{1,7},{3,1},{5,3},{7,5},{8,14},{10,8},{12,... | collective-permute-start | bytes 1572872 | tf_op jit(solution)/shard_map/ppermute | solution.py:26
  (9 other events, 118.5 us)
